TPU v7x, 32 devices: a whole 2x2x4 slice. The times are simulated.
32 devices in a mesh: sp: 8 (over z, x), tp: 4 (over y, core).
Axes of the slice: x: 2, y: 2, z: 4, core: 2. Of those that a mesh axis runs over, the one named last changes fastest.
Arguments:
- tokens: bfloat16 [8192, 2048], P('sp'), may hold values from -6 to 6
- pre_gain: float32 [2048], replicated, may hold values from 0.1 to 1.9
- w_query: bfloat16 [2048, 2048], P(None, 'tp'), may hold values from -0.125 to 0.125
- w_key: bfloat16 [2048, 2048], P(None, 'tp'), may hold values from -0.125 to 0.125
- w_value: bfloat16 [2048, 2048], P(None, 'tp'), may hold values from -0.125 to 0.125
- memory_output_gate_weight: bfloat16 [2048, 2048], P(None, 'tp'), may hold values from -0.125 to 0.125
- w_input_gate: bfloat16 [2048, 8], replicated, may hold values from -0.125 to 0.125
- w_forget_gate: bfloat16 [2048, 8], replicated, may hold values from -0.125 to 0.125
- input_bias: float32 [8], replicated, may hold values from -3 to 220
- forget_bias: float32 [8], replicated, may hold values from 3.9 to 12.4
- forget_extra: float32 [8192, 8], P('sp', 'tp'), may hold values from -1.5 to 0
- initial_memory: float32 [8, 256, 256], P('tp', 'sp'), may hold values from -2048 to 2048
- initial_normal: float32 [8, 256], P('tp', 'sp'), may hold values from -2048 to 2048
- memory_gain: float32 [2048], replicated, may hold values from 0.1 to 1.9
- w_pool_input: bfloat16 [2048, 1024], P(None, 'tp'), may hold values from -0.125 to 0.125
- w_pool_gate: bfloat16 [2048, 1024], P(None, 'tp'), may hold values from -0.125 to 0.125
- pool_mix: bfloat16 [8, 128, 128], replicated, may hold values from -0.5 to 0.5
- pool_gain: float32 [1024], replicated, may hold values from 0.1 to 1.9
- w_out_memory: bfloat16 [2048, 2048], P('tp'), may hold values from -0.109375 to 0.109375
- w_out_pool: bfloat16 [1024, 2048], P('tp'), may hold values from -0.109375 to 0.109375
- post_gain: float32 [2048], replicated, may hold values from 0.1 to 1.9
Outputs:
- layer_out: bfloat16 [8192, 2048], P(('sp', 'tp'))
All inputs are finite; a program needn't handle non-finite values.
Results may differ from a plain program's by a relative error of at most 0.018.
The roundings to bfloat16 on the way count: a program that leaves them out, or rounds other values in their place, can miss the bound.
Values may be sent and summed in bfloat16 or wider, within the bound.
A program may use at most 128 MiB of HBM per device.

v0:
```python
import functools

import jax
import jax.numpy as jnp
from jax import lax
from jax.experimental import pallas as pl
from jax.experimental.pallas import tpu as pltpu
from jax.sharding import PartitionSpec as P

HEAD_DIM = 256
GROUP_DIM = 128
WIDEST = 256
TILE = 256
CHUNKS = 2
EPS = 1e-06
FLOOR = -1e30
F32 = jnp.float32
BF16 = jnp.bfloat16
MESH = pl.DeviceIdType.MESH


def dot(a, b):
    return jnp.dot(a, b, preferred_element_type=F32)


def silu(x):
    return x / (1.0 + jnp.exp(-x))


def kernel(
    n_sp,
    n_tp,
    tokens_hbm,
    gain_ref,
    wq_hbm,
    wk_hbm,
    wv_hbm,
    wg_hbm,
    w_in_ref,
    w_forget_ref,
    b_in_ref,
    b_forget_ref,
    extra_ref,
    init_ref,
    normal_ref,
    mem_gain_ref,
    wpi_hbm,
    wpg_hbm,
    mix_ref,
    pool_gain_ref,
    wom_hbm,
    wop_hbm,
    post_ref,
    out_ref,
    tokens,
    wq,
    wk,
    wv,
    wg,
    wpi,
    wpg,
    wom,
    wop,
    normed,
    q_ref,
    k_ref,
    v_ref,
    gate_ref,
    pgate_ref,
    ext_ref,
    pool_ref,
    rows_ref,
    cols_ref,
    num_ref,
    den_ref,
    max_ref,
    s_send,
    s_recv,
    a_send,
    a_recv,
    e_send,
    e_recv,
    sq_send,
    sq_recv,
    scale_ref,
    sib_send,
    sib_recv,
    own_ref,
    link_send,
    link_recv,
    gates_w_ref,
    gates_b_ref,
    raw_ref,
    start_ref,
    local_sem,
    s_sems,
    a_sems,
    e_sems,
    halo_sems,
    sq_sems,
    sib_sems,
    link_sems,
):
    T, D = tokens.shape
    H = q_ref.shape[0]
    G = pool_ref.shape[1] // GROUP_DIM
    sp = lax.axis_index("sp")
    tp = lax.axis_index("tp")
    head_scale = HEAD_DIM ** (-0.5)
    tiles = T // TILE

    loads = {}
    for slot, (name, src, dst) in enumerate(
        [
            ("tokens", tokens_hbm, tokens),
            ("wk", wk_hbm, wk),
            ("wv", wv_hbm, wv),
            ("wpi", wpi_hbm, wpi),
            ("wq", wq_hbm, wq),
            ("wg", wg_hbm, wg),
            ("wpg", wpg_hbm, wpg),
            ("wop", wop_hbm, wop),
            ("wom", wom_hbm, wom),
        ]
    ):
        loads[name] = pltpu.make_async_copy(src, dst, local_sem.at[slot])
        loads[name].start()

    barrier = pltpu.get_barrier_semaphore()
    for step in range(1, n_sp):
        pl.semaphore_signal(
            barrier, inc=1, device_id={"sp": lax.rem(sp + step, n_sp)}, device_id_type=MESH
        )
    for step in range(1, n_tp):
        pl.semaphore_signal(
            barrier, inc=1, device_id={"tp": lax.rem(tp + step, n_tp)}, device_id_type=MESH
        )

    def remote(src, dst, sems, slot, axis, peer):
        return pltpu.make_async_remote_copy(
            src_ref=src,
            dst_ref=dst,
            send_sem=sems.at[0, slot],
            recv_sem=sems.at[1, slot],
            device_id={axis: peer},
            device_id_type=MESH,
        )

    def by_tile(body, size=TILE):
        def step(index, carry):
            body(pl.ds(pl.multiple_of(index * size, size), size))
            return carry

        lax.fori_loop(0, T // size, step, 0)

    heads = w_in_ref.shape[1]
    gates_w_ref[...] = jnp.zeros_like(gates_w_ref)
    gates_w_ref[:, 0:heads] = w_in_ref[...]
    gates_w_ref[:, heads : 2 * heads] = w_forget_ref[...]
    gates_b_ref[...] = jnp.zeros_like(gates_b_ref)
    gates_b_ref[:, 0:heads] = b_in_ref[...]
    gates_b_ref[:, heads : 2 * heads] = b_forget_ref[...]

    loads["tokens"].wait()

    def norm_tile(rows):
        x = tokens[rows, :].astype(F32)
        scale = lax.rsqrt(jnp.mean(x * x, axis=-1, keepdims=True) + EPS)
        normed[rows, :] = (x * scale * gain_ref[...]).astype(BF16)

    def early_products(t):
        rows = pl.ds(t * TILE, TILE)
        cols_ref[rows, :] = dot(normed[rows, :], gates_w_ref[...]) + gates_b_ref[...]
        cols_ref[rows, 2 * heads : 2 * heads + H] = extra_ref[rows, :]
        keys = dot(normed[rows, :], wk[...])
        for h in range(H):
            k_ref[h, rows, :] = keys[:, h * HEAD_DIM : (h + 1) * HEAD_DIM].astype(BF16)

    for t in range(tiles + 1):
        if t == 1:
            loads["wk"].wait()
        if t < tiles:
            for sub in range(0, TILE, 64):
                norm_tile(pl.ds(t * TILE + sub, 64))
        if t > 0:
            early_products(t - 1)
    tri = (
        lax.broadcasted_iota(jnp.int32, (TILE, TILE), 0)
        <= lax.broadcasted_iota(jnp.int32, (TILE, TILE), 1)
    ).astype(F32)
    rows_ref[...] = jnp.zeros_like(rows_ref)
    carry = jnp.zeros((8, 1), F32)
    for t in range(tiles):
        span = pl.ds(t * TILE, TILE)
        raw_ref[:, span] = cols_ref[span, :].T
        own_rows = [raw_ref[pl.ds(heads + tp * H + h, 1), span] for h in range(H)]
        added = [raw_ref[2 * heads + h : 2 * heads + h + 1, span] for h in range(H)]
        spare = [jnp.zeros((8 - H, TILE), F32)]
        raw = jnp.concatenate(own_rows + spare, axis=0)
        log_keep = jnp.minimum(raw, 0.0) - jnp.log1p(jnp.exp(-jnp.abs(raw)))
        log_keep = log_keep + jnp.concatenate(added + spare, axis=0)
        run = carry + jnp.dot(
            log_keep, tri, preferred_element_type=F32, precision=lax.Precision.HIGHEST
        )
        carry = run[:, TILE - 1 : TILE]
        for h in range(H):
            keep = run[h : h + 1]
            rows_ref[h : h + 1, span] = raw_ref[pl.ds(tp * H + h, 1), span] - keep
            rows_ref[H + h : H + h + 1, span] = keep
    for t in range(tiles):
        span = pl.ds(t * TILE, TILE)
        cols_ref[span, :] = rows_ref[:, span].T

    def project(name, weight, store):
        loads[name].wait()

        def tile(rows):
            store(rows, dot(normed[rows, :], weight[...]))

        by_tile(tile)

    def heads_to(ref):
        def store(rows, value):
            for h in range(H):
                ref[h, rows, :] = value[:, h * HEAD_DIM : (h + 1) * HEAD_DIM].astype(ref.dtype)

        return store

    project("wv", wv, heads_to(v_ref))

    part = HEAD_DIM // n_sp
    a_send[...] = jnp.zeros_like(a_send)
    for h in range(H):
        a_max = jnp.max(rows_ref[h : h + 1, :], axis=-1, keepdims=True)
        total = rows_ref[H + h : H + h + 1, T - 1 : T]
        state = jnp.zeros((HEAD_DIM, HEAD_DIM), F32)
        normal = jnp.zeros((1, HEAD_DIM), F32)
        for t in range(tiles):
            span = pl.ds(t * TILE, TILE)
            weight = jnp.exp(cols_ref[span, h : h + 1] - a_max)
            kw = weight * k_ref[h, span, :].astype(F32)
            normal = normal + jnp.sum(kw, axis=0, keepdims=True)
            state = state + lax.dot_general(
                kw.astype(BF16),
                v_ref[h, span, :],
                (((0,), (0,)), ((), ())),
                preferred_element_type=F32,
            )
        s_send[:, h] = state.reshape(n_sp, part, HEAD_DIM).astype(s_send.dtype)
        a_send[4 * h : 4 * h + 1, :] = jnp.broadcast_to(total + a_max, (1, HEAD_DIM))
        a_send[4 * h + 1 : 4 * h + 2, :] = jnp.broadcast_to(total, (1, HEAD_DIM))
        a_send[4 * h + 2 : 4 * h + 3, :] = normal
        a_send[4 * h + 3 : 4 * h + 4, 0:part] = normal_ref[h : h + 1, :]

    pl.semaphore_wait(barrier, n_sp - 1 + n_tp - 1)
    first = []
    for step in range(1, n_sp):
        peer = lax.rem(sp + step, n_sp)
        first.append(remote(s_send.at[peer], s_recv.at[sp], s_sems, step, "sp", peer))
        first.append(remote(a_send, a_recv.at[sp], a_sems, step, "sp", peer))
    for copy in first:
        copy.start()
    s_recv[sp] = s_send[sp]
    a_recv[sp] = a_send[...]

    def store_pool(rows, value):
        ext_ref[pl.ds(pl.multiple_of(rows.start + WIDEST, TILE), TILE), :] = value.astype(BF16)

    project("wpi", wpi, store_pool)
    halo = remote(
        ext_ref.at[pl.ds(T, WIDEST)],
        ext_ref.at[pl.ds(0, WIDEST)],
        halo_sems,
        0,
        "sp",
        lax.rem(sp + 1, n_sp),
    )
    halo.start()
    project("wq", wq, heads_to(q_ref))
    project("wg", wg, heads_to(gate_ref))

    for copy in first:
        copy.wait()
    enter_max, enter_normal = [], []
    for h in range(H):
        state = init_ref[h].astype(F32)
        for j in range(n_sp):
            start_ref[h : h + 1, j * part : (j + 1) * part] = a_recv[j, 4 * h + 3 : 4 * h + 4, 0:part]
        normal = start_ref[h : h + 1, :]
        stab = jnp.zeros((1, HEAD_DIM), F32)
        my_stab, my_normal = stab, normal
        for j in range(n_sp):
            e_send[j, h] = state.astype(e_send.dtype)
            my_stab = jnp.where(sp == j, stab, my_stab)
            my_normal = jnp.where(sp == j, normal, my_normal)
            late = a_recv[j, 4 * h : 4 * h + 1, :]
            keep = a_recv[j, 4 * h + 1 : 4 * h + 2, :]
            joint = jnp.maximum(late, keep + stab)
            early_factor = jnp.exp(keep + stab - joint)
            late_factor = jnp.exp(late - joint)
            state = state * early_factor + s_recv[j, h].astype(F32) * late_factor
            normal = normal * early_factor + a_recv[j, 4 * h + 2 : 4 * h + 3, :] * late_factor
            stab = joint
        enter_max.append(my_stab[:, 0:1])
        enter_normal.append(my_normal)
    second = []
    for step in range(1, n_sp):
        peer = lax.rem(sp + step, n_sp)
        second.append(remote(e_send.at[peer], e_recv.at[sp], e_sems, step, "sp", peer))
    for copy in second:
        copy.start()
    e_recv[sp] = e_send[sp]

    for h in range(H):
        for t in range(tiles):
            span = pl.ds(t * TILE, TILE)
            width = (t + 1) * TILE
            decayed = cols_ref[span, H + h : H + h + 1] + rows_ref[h : h + 1, 0:width]
            causal = (
                lax.broadcasted_iota(jnp.int32, (TILE, width), 0) + t * TILE
                >= lax.broadcasted_iota(jnp.int32, (TILE, width), 1)
            )
            decayed = jnp.where(causal, decayed, FLOOR)
            row_max = jnp.max(decayed, axis=-1, keepdims=True)
            scores = lax.dot_general(
                q_ref[h, span, :],
                k_ref[h, 0:width, :],
                (((1,), (1,)), ((), ())),
                preferred_element_type=F32,
            )
            weights = jnp.exp(decayed - row_max) * scores * head_scale
            den_ref[h, span, :] = jnp.sum(weights, axis=-1, keepdims=True)
            max_ref[h, span, :] = row_max
            num_ref[h, span, :] = dot(weights.astype(BF16), v_ref[h, 0:width, :])

    def store_gate(rows, value):
        pgate_ref[rows, :] = value

    project("wpg", wpg, store_gate)
    halo.wait()
    for g in range(G):
        window = jnp.left_shift(2, tp * G + g)
        offset = (
            lax.broadcasted_iota(jnp.int32, (TILE, TILE + WIDEST), 0)
            + WIDEST
            - lax.broadcasted_iota(jnp.int32, (TILE, TILE + WIDEST), 1)
        )
        band = jnp.where((offset >= 0) & (offset < window), 1.0, 0.0).astype(BF16)
        lanes = slice(g * GROUP_DIM, (g + 1) * GROUP_DIM)
        for t in range(tiles):
            span = pl.ds(t * TILE, TILE)
            here = ext_ref[t * TILE + WIDEST : (t + 1) * TILE + WIDEST, lanes]
            before = ext_ref[t * TILE : t * TILE + WIDEST, lanes]
            if t == 0:
                before = jnp.where(sp > 0, before.astype(F32), 0.0).astype(BF16)
            sums = dot(band[:, :WIDEST], before) + dot(band[:, WIDEST:], here)
            position = lax.broadcasted_iota(jnp.int32, (TILE, 1), 0) + (sp * T + t * TILE + 1)
            counts = jnp.minimum(position, window).astype(F32)
            pooled = (sums / counts - here.astype(F32)).astype(BF16)
            mixed = dot(pooled, mix_ref[tp * G + g])
            pool_ref[span, lanes] = (
                mixed * pool_gain_ref[:, pl.ds(pl.multiple_of((tp * G + g) * GROUP_DIM, GROUP_DIM), GROUP_DIM)] * silu(pgate_ref[span, lanes])
            ).astype(BF16)

    for copy in second:
        copy.wait()
    for t in range(tiles):
        span = pl.ds(t * TILE, TILE)
        squares = jnp.zeros((TILE, 1), F32)
        for h in range(H):
            state = e_recv[:, h].reshape(HEAD_DIM, HEAD_DIM).astype(BF16)
            queries = q_ref[h, span, :]
            carried = cols_ref[span, H + h : H + h + 1] + enter_max[h]
            row_max = max_ref[h, span, :]
            joint = jnp.maximum(row_max, carried)
            local_weight = jnp.exp(row_max - joint)
            carry_weight = jnp.exp(carried - joint) * head_scale
            numerator = num_ref[h, span, :] * local_weight + carry_weight * dot(queries, state)
            denominator = den_ref[h, span, :] * local_weight + carry_weight * jnp.sum(
                queries.astype(F32) * enter_normal[h], axis=-1, keepdims=True
            )
            memory = numerator / jnp.maximum(jnp.abs(denominator), jnp.exp(-joint))
            num_ref[h, span, :] = memory
            squares = squares + jnp.sum(memory * memory, axis=-1, keepdims=True)
        sq_send[:, span] = jnp.broadcast_to(squares, (TILE, 128)).T[0:8]

    third = []
    for step in range(1, n_tp):
        peer = lax.rem(tp + step, n_tp)
        third.append(remote(sq_send, sq_recv.at[step], sq_sems, step, "tp", peer))
    for copy in third:
        copy.start()
    loads["wop"].wait()
    loads["wom"].wait()
    for copy in third:
        copy.wait()
    for t in range(tiles):
        span = pl.ds(t * TILE, TILE)
        total = sq_send[0:1, span]
        for step in range(1, n_tp):
            total = total + sq_recv[step, 0:1, span]
        scale = lax.rsqrt(total / (HEAD_DIM * H * n_tp) + EPS)
        scale_ref[span, :] = jnp.broadcast_to(scale, (128, TILE)).T

    chips = n_tp // 2
    chip, core = tp // 2, lax.rem(tp, 2)
    sibling = chip * 2 + 1 - core
    block = T // n_tp
    size = block // CHUNKS

    def memory_out(rows):
        parts = []
        for h in range(H):
            lanes = pl.ds(pl.multiple_of((tp * H + h) * HEAD_DIM, HEAD_DIM), HEAD_DIM)
            parts.append(
                (
                    num_ref[h, rows, :]
                    * scale_ref[rows, 0:1]
                    * mem_gain_ref[:, lanes]
                    * silu(gate_ref[h, rows, :])
                ).astype(BF16)
            )
        return parts[0] if H == 1 else jnp.concatenate(parts, axis=1)

    links, siblings = [], []
    for j in range(1, chips + 1):
        target = lax.rem(chip + j, chips)
        for n in range(CHUNKS):
            slot = (j - 1) * CHUNKS + n
            theirs = pl.ds(
                pl.multiple_of((target * 2 + 1 - core) * block + n * size, size), size
            )
            ours = pl.ds(pl.multiple_of((target * 2 + core) * block + n * size, size), size)
            lhs_memory = jnp.concatenate([memory_out(theirs), memory_out(ours)], axis=0)
            lhs_pool = jnp.concatenate([pool_ref[theirs, :], pool_ref[ours, :]], axis=0)
            both = (dot(lhs_memory, wom[...]) + dot(lhs_pool, wop[...])).astype(BF16)
            sib_send[slot] = both[:size]
            own_ref[slot] = both[size:]
            copy = remote(
                sib_send.at[slot], sib_recv.at[slot], sib_sems, slot, "tp", sibling
            )
            copy.start()
            siblings.append(copy)
            if j < chips:
                copy.wait_recv()
                link_send[slot] = (
                    own_ref[slot].astype(F32) + sib_recv[slot].astype(F32)
                ).astype(BF16)
                hop = remote(
                    link_send.at[slot],
                    link_recv.at[slot],
                    link_sems,
                    slot,
                    "tp",
                    target * 2 + core,
                )
                hop.start()
                links.append(hop)
    for n in range(CHUNKS):
        slot = (chips - 1) * CHUNKS + n
        siblings[slot].wait_recv()
        total = own_ref[slot].astype(F32) + sib_recv[slot].astype(F32)
        for j in range(1, chips):
            other = (j - 1) * CHUNKS + n
            links[other].wait_recv()
            total = total + link_recv[other].astype(F32)
        scale = lax.rsqrt(jnp.mean(total * total, axis=-1, keepdims=True) + EPS)
        out_ref[pl.ds(n * size, size), :] = (total * scale * post_ref[...]).astype(BF16)
    for copy in siblings + links:
        copy.wait_send()


def body(
    n_sp,
    n_tp,
    tokens,
    pre_gain,
    w_query,
    w_key,
    w_value,
    memory_output_gate_weight,
    w_input_gate,
    w_forget_gate,
    input_bias,
    forget_bias,
    forget_extra,
    initial_memory,
    initial_normal,
    memory_gain,
    w_pool_input,
    w_pool_gate,
    pool_mix,
    pool_gain,
    w_out_memory,
    w_out_pool,
    post_gain,
):
    T, D = tokens.shape
    MW = w_query.shape[1]
    PW = w_pool_input.shape[1]
    H = MW // HEAD_DIM
    G = PW // GROUP_DIM
    part = initial_normal.shape[1]
    wire = BF16 if part % 16 == 0 else F32
    chips = n_tp // 2
    block = T // n_tp
    slots = chips * CHUNKS
    size = block // CHUNKS
    hbm = pl.BlockSpec(memory_space=pl.ANY)
    vmem = pl.BlockSpec(memory_space=pltpu.VMEM)
    V = pltpu.VMEM
    dma = pltpu.SemaphoreType.DMA
    return pl.pallas_call(
        functools.partial(kernel, n_sp, n_tp),
        out_shape=jax.ShapeDtypeStruct((block, D), BF16),
        in_specs=[hbm, vmem, hbm, hbm, hbm, hbm, vmem, vmem, vmem, vmem, vmem, vmem, vmem, vmem]
        + [hbm, hbm, vmem, vmem, hbm, hbm, vmem],
        out_specs=vmem,
        scratch_shapes=[
            V((T, D), BF16),
            V((D, MW), BF16),
            V((D, MW), BF16),
            V((D, MW), BF16),
            V((D, MW), BF16),
            V((D, PW), BF16),
            V((D, PW), BF16),
            V((MW, D), BF16),
            V((PW, D), BF16),
            V((T, D), BF16),
            V((H, T, HEAD_DIM), BF16),
            V((H, T, HEAD_DIM), BF16),
            V((H, T, HEAD_DIM), BF16),
            V((H, T, HEAD_DIM), F32),
            V((T, PW), F32),
            V((T + WIDEST, PW), BF16),
            V((T, PW), BF16),
            V((128, T), F32),
            V((T, 128), F32),
            V((H, T, HEAD_DIM), F32),
            V((H, T, 1), F32),
            V((H, T, 1), F32),
            V((n_sp, H, part, HEAD_DIM), wire),
            V((n_sp, H, part, HEAD_DIM), wire),
            V((8, HEAD_DIM), F32),
            V((n_sp, 8, HEAD_DIM), F32),
            V((n_sp, H, part, HEAD_DIM), wire),
            V((n_sp, H, part, HEAD_DIM), wire),
            V((8, T), F32),
            V((n_tp, 8, T), F32),
            V((T, 128), F32),
            V((slots, size, D), BF16),
            V((slots, size, D), BF16),
            V((slots, size, D), BF16),
            V((slots, size, D), BF16),
            V((slots, size, D), BF16),
            V((D, 128), BF16),
            V((1, 128), F32),
            V((128, T), F32),
            V((8, HEAD_DIM), F32),
            dma((9,)),
            dma((2, n_sp)),
            dma((2, n_sp)),
            dma((2, n_sp)),
            dma((2, 1)),
            dma((2, n_tp)),
            dma((2, slots)),
            dma((2, slots)),
        ],
        compiler_params=pltpu.CompilerParams(
            collective_id=0, has_side_effects=True, vmem_limit_bytes=60 * 1024 * 1024
        ),
    )(
        tokens,
        pre_gain[None],
        w_query,
        w_key,
        w_value,
        memory_output_gate_weight,
        w_input_gate,
        w_forget_gate,
        input_bias[None],
        forget_bias[None],
        forget_extra,
        initial_memory,
        initial_normal,
        memory_gain[None],
        w_pool_input,
        w_pool_gate,
        pool_mix,
        pool_gain[None],
        w_out_memory,
        w_out_pool,
        post_gain[None],
    )


def solution(mesh):
    in_specs = (
        P("sp", None),
        P(),
        P(None, "tp"),
        P(None, "tp"),
        P(None, "tp"),
        P(None, "tp"),
        P(),
        P(),
        P(),
        P(),
        P("sp", "tp"),
        P("tp", "sp", None),
        P("tp", "sp"),
        P(),
        P(None, "tp"),
        P(None, "tp"),
        P(),
        P(),
        P("tp", None),
        P("tp", None),
        P(),
    )
    out_specs = P(("sp", "tp"), None)
    sizes = dict(mesh.shape)
    run = functools.partial(body, sizes["sp"], sizes["tp"])
    return jax.shard_map(run, mesh=mesh, in_specs=in_specs, out_specs=out_specs, check_vma=False)
```

profile of v0, /device:TPU:0, one launch (start us, length us, event | category | flops | bytes accessed | tf_op | source)
XLA Modules:
  0.0 78.5 jit_solution(615997900403185305)
XLA Ops:
  0.0 1.8 %copy.22.w_in_ref = bf16[2048,8]{1,0:T(8,128)(2,1)} copy(bf16[2048,8]{0,1:T(8,128)(2,1)} %param.27) | data formatting | bytes 65536 | tf_op args[6]
  1.8 1.8 %copy.23.w_forget_ref = bf16[2048,8]{1,0:T(8,128)(2,1)} copy(bf16[2048,8]{0,1:T(8,128)(2,1)} %param.28) | data formatting | bytes 65536 | tf_op args[7]
  3.5 1.7 %copy.24.extra_ref = f32[1024,2]{1,0:T(8,128)} copy(f32[1024,2]{0,1:T(2,128)} %param.31) | data formatting | bytes 16384 | tf_op args[10]
  5.3 70.9 %shard_map.199 = bf16[256,2048]{1,0:T(8,128)(2,1)} custom-call(bf16[1024,2048]{1,0:T(8,128)(2,1)} %tokens_hbm.1, f32[1,2048]{1,0:T(1,128)} %bitcast.6, bf16[2048,512]{1,0:T(8,128)(2,1)} %wq_hbm.1, bf16[2048,512]{1,0:T(8,128)(2,1)} %wk_hbm.1, bf16[2048,512]{1,0:T(8,128)(2,1)} %wv_hbm.1, bf16[2048,512]{1,0:T(8,128)(2,1)} %wg_hbm.1, ...), custom_call_target="tpu_custom_call" | custom-call | tf_op jit(solution)/shard_map/pallas_call | solution.py:513
  76.2 2.3 %copy.26 = bf16[256,2048]{1,0:T(8,128)(2,1)} copy(bf16[256,2048]{1,0:T(8,128)(2,1)} %shard_map.199) | data formatting | bytes 2097152
where the time goes:
time: 79.5 us; the launch traced here: 78.5 us
  Pallas kernels  70.9 us (89%)
  local copies, waits for them, and re-layouts  7.58 us (10%)
    pallas_call x1, Pallas kernels, body(): pl.pallas_call(functools.partial(kernel, n_sp, n_tp), out_shape=jax.Shape...  70.9 us
    unnamed x4, local copies, waits for them, and re-layouts  7.58 us

commit v1 on v0

v1 whole, which is shorter than its diff:
```python
import functools
import types

import jax
import jax.numpy as jnp
from jax import lax
from jax.experimental import pallas as pl
from jax.experimental.pallas import tpu as pltpu
from jax.sharding import PartitionSpec as P

HEAD_DIM = 256
GROUP_DIM = 128
WIDEST = 256
TILE = 256
CHUNKS = 4
QUAD = 4
SUB = 64
EPS = 1e-06
FLOOR = -1e30
F32 = jnp.float32
BF16 = jnp.bfloat16
MESH = pl.DeviceIdType.MESH
INPUTS = 21


def dot(a, b):
    return jnp.dot(a, b, preferred_element_type=F32)


def dot_t(a, b):
    return lax.dot_general(a, b, (((1,), (1,)), ((), ())), preferred_element_type=F32)


def silu(x):
    return x / (1.0 + jnp.exp(-x))


def kernel(n_sp, n_tp, names, *refs):
    (
        tokens_hbm,
        gain_hbm,
        wq_hbm,
        wk_hbm,
        wv_hbm,
        wg_hbm,
        w_in_hbm,
        w_forget_hbm,
        b_in_hbm,
        b_forget_hbm,
        extra_hbm,
        init_hbm,
        normal_hbm,
        mem_gain_hbm,
        wpi_hbm,
        wpg_hbm,
        mix_hbm,
        pool_gain_hbm,
        wom_hbm,
        wop_hbm,
        post_hbm,
    ) = refs[:INPUTS]
    out_hbm = refs[INPUTS]
    r = types.SimpleNamespace(**dict(zip(names, refs[INPUTS + 1 :])))
    T, D = r.tokens.shape
    H = r.q.shape[0]
    G = r.mix.shape[0]
    heads = r.w_in.shape[0]
    sp = lax.axis_index("sp")
    tp = lax.axis_index("tp")
    head_scale = HEAD_DIM ** (-0.5)
    tiles = T // TILE
    quad = r.e_recv.shape[1]
    rows_own = HEAD_DIM // quad
    quads = n_sp // quad
    my_quad, my_slot = sp // quad, lax.rem(sp, quad)
    part = HEAD_DIM // n_sp

    mem_lanes = pl.ds(pl.multiple_of(tp * H * HEAD_DIM, HEAD_DIM), H * HEAD_DIM)
    pool_lanes = pl.ds(pl.multiple_of(tp * G * GROUP_DIM, GROUP_DIM), G * GROUP_DIM)
    loads = {}

    def load(name, src, dst):
        loads[name] = pltpu.make_async_copy(src, dst, r.local_sem.at[len(loads)])
        loads[name].start()

    load("gain", gain_hbm, r.gain)

    def load_tokens(t):
        span = pl.ds(t * TILE, TILE)
        load(("tokens", t), tokens_hbm.at[span], r.tokens.at[span])

    def load_head(name, source, target, h):
        lanes = pl.ds(h * HEAD_DIM, HEAD_DIM)
        load((name, h), source.at[:, lanes], target.at[:, lanes])

    for t in range(tiles // 2):
        load_tokens(t)
    load("w_in", w_in_hbm, r.w_in)
    load("w_forget", w_forget_hbm, r.w_forget)
    load("b_in", b_in_hbm, r.b_in)
    load("b_forget", b_forget_hbm, r.b_forget)
    load_head("wk", wk_hbm, r.wk, 0)
    for t in range(tiles // 2, tiles):
        load_tokens(t)
    load_head("wv", wv_hbm, r.wv, 0)
    load("extra", extra_hbm, r.extra)
    load("normal", normal_hbm, r.normal)
    for h in range(1, H):
        load_head("wk", wk_hbm, r.wk, h)
        load_head("wv", wv_hbm, r.wv, h)
    load("wpi", wpi_hbm, r.wpi)
    load("wq", wq_hbm, r.wq)
    load("wpg", wpg_hbm, r.wpg)
    load("wg", wg_hbm, r.wg)
    load("mix", mix_hbm.at[pl.ds(tp * G, G)], r.mix)
    load("pool_gain", pool_gain_hbm.at[:, pool_lanes], r.pool_gain)
    load("mem_gain", mem_gain_hbm.at[:, mem_lanes], r.mem_gain)
    load("wop", wop_hbm, r.wop)
    load("wom", wom_hbm, r.wom)
    load("post", post_hbm, r.post)

    barrier = pltpu.get_barrier_semaphore()
    for step in range(1, n_sp):
        pl.semaphore_signal(
            barrier, inc=1, device_id={"sp": lax.rem(sp + step, n_sp)}, device_id_type=MESH
        )
    for step in range(1, n_tp):
        pl.semaphore_signal(
            barrier, inc=1, device_id={"tp": lax.rem(tp + step, n_tp)}, device_id_type=MESH
        )

    def remote(src, dst, send_sem, recv_sem, axis, peer):
        return pltpu.make_async_remote_copy(
            src_ref=src,
            dst_ref=dst,
            send_sem=send_sem,
            recv_sem=recv_sem,
            device_id={axis: peer},
            device_id_type=MESH,
        )

    r.gates_w[...] = jnp.zeros_like(r.gates_w)
    r.gates_b[...] = jnp.zeros_like(r.gates_b)
    r.rows[...] = jnp.zeros_like(r.rows)
    r.a_send[...] = jnp.zeros_like(r.a_send)
    loads["gain"].wait()
    loads["tokens", 0].wait()

    def norm_tile(rows):
        x = r.tokens[rows, :].astype(F32)
        scale = lax.rsqrt(jnp.mean(x * x, axis=-1, keepdims=True) + EPS)
        r.normed[rows, :] = (x * scale * r.gain[...]).astype(BF16)

    def head_lanes(h):
        return slice(h * HEAD_DIM, (h + 1) * HEAD_DIM)

    def whole(ref, h):
        return lambda rows, value: ref.__setitem__((h, rows), value.astype(ref.dtype))

    def gates_product(rows):
        r.cols[rows, :] = dot_t(r.normed[rows, :], r.gates_w[...]) + r.gates_b[...]

    def product(weight, lanes, rows, store):
        store(rows, dot(r.normed[rows, :], weight[:, lanes]))

    per_owner = n_sp // quad
    owner = sp // per_owner
    turn = lax.rem(sp, per_owner)
    init_place = r.init.at[:, pl.ds(pl.multiple_of(turn * part, part), part), :]
    init_copy = remote(
        init_hbm, init_place, r.init_sems.at[per_owner], r.init_sems.at[turn], "sp", owner
    )
    init_local = pltpu.make_async_copy(init_hbm, init_place, r.init_sems.at[per_owner])

    def send_init():
        pl.semaphore_wait(barrier, n_sp - 1 + n_tp - 1)

        @pl.when(owner != sp)
        def _():
            init_copy.start()

        @pl.when(owner == sp)
        def _():
            init_local.start()

    half = tiles // 2
    for t in range(half):
        if t > 0:
            loads["tokens", t].wait()
        for sub in range(0, TILE, SUB):
            norm_tile(pl.ds(t * TILE + sub, SUB))
    for name in ("w_in", "w_forget", "b_in", "b_forget", ("wk", 0)):
        loads[name].wait()
    r.gates_w[0:heads, :] = r.w_in[...]
    r.gates_w[heads : 2 * heads, :] = r.w_forget[...]
    r.gates_b[:, 0:heads] = r.b_in[...]
    r.gates_b[:, heads : 2 * heads] = r.b_forget[...]
    for t in range(half, tiles):
        loads["tokens", t].wait()

    def early_products(rows):
        gates_product(rows)
        product(r.wk, head_lanes(0), rows, whole(r.k, 0))

    pieces = (slice(0, half * TILE), slice(half * TILE, T))
    early_products(pieces[0])
    for t in range(half, tiles):
        for sub in range(0, TILE, SUB):
            norm_tile(pl.ds(t * TILE + sub, SUB))
    for name in (("wv", 0), "extra", "normal"):
        loads[name].wait()
    early_products(pieces[1])
    send_init()
    for rows in pieces:
        product(r.wv, head_lanes(0), rows, whole(r.v, 0))

    tri = (
        lax.broadcasted_iota(jnp.int32, (TILE, TILE), 0)
        <= lax.broadcasted_iota(jnp.int32, (TILE, TILE), 1)
    ).astype(F32)
    carry = jnp.zeros((8, 1), F32)
    for t in range(tiles):
        span = pl.ds(t * TILE, TILE)
        r.raw[:, span] = r.cols[span, :].T
        own_rows = [r.raw[pl.ds(heads + tp * H + h, 1), span] for h in range(H)]
        added = [r.extra[h : h + 1, span] for h in range(H)]
        spare = [jnp.zeros((8 - H, TILE), F32)]
        raw = jnp.concatenate(own_rows + spare, axis=0)
        log_keep = jnp.minimum(raw, 0.0) - jnp.log1p(jnp.exp(-jnp.abs(raw)))
        log_keep = log_keep + jnp.concatenate(added + spare, axis=0)
        run = carry + jnp.dot(
            log_keep, tri, preferred_element_type=F32, precision=lax.Precision.HIGHEST
        )
        carry = run[:, TILE - 1 : TILE]
        for h in range(H):
            keep = run[h : h + 1]
            r.rows[h : h + 1, span] = r.raw[pl.ds(tp * H + h, 1), span] - keep
            r.rows[H + h : H + h + 1, span] = keep
    for t in range(tiles):
        span = pl.ds(t * TILE, TILE)
        r.cols[span, :] = r.rows[:, span].T

    def a_copy(h, step):
        peer = lax.rem(sp + step, n_sp)
        return remote(
            r.a_send.at[h], r.a_recv.at[sp, h], r.a_sems.at[0, h, step], r.a_sems.at[1, h, step], "sp", peer
        )

    def s_copy(h, step):
        peer = lax.rem(my_slot + step, quad)
        return remote(
            r.s_send.at[h, peer],
            r.s_recv.at[h, my_slot],
            r.s_sems.at[0, h, step],
            r.s_sems.at[1, h, step],
            "sp",
            my_quad * quad + peer,
        )

    def e_copy(h, step):
        peer = lax.rem(my_slot + step, quad)
        return remote(
            r.e_send.at[h, peer],
            r.e_recv.at[h, my_slot],
            r.e_sems.at[0, h, step],
            r.e_sems.at[1, h, step],
            "sp",
            my_quad * quad + peer,
        )

    def t_copy(h):
        return remote(
            r.t_send.at[h],
            r.t_recv.at[h],
            r.t_sems.at[0, h],
            r.t_sems.at[1, h],
            "sp",
            lax.rem(sp + quad, n_sp),
        )

    for h in range(H):
        if h > 0:
            loads["wk", h].wait()
            loads["wv", h].wait()
            product(r.wk, head_lanes(h), slice(0, T), whole(r.k, h))
            product(r.wv, head_lanes(h), slice(0, T), whole(r.v, h))
        a_max = jnp.max(r.rows[h : h + 1, :], axis=-1, keepdims=True)
        total = r.rows[H + h : H + h + 1, T - 1 : T]
        state = jnp.zeros((HEAD_DIM, HEAD_DIM), F32)
        normal = jnp.zeros((1, HEAD_DIM), F32)
        for t in range(tiles):
            span = pl.ds(t * TILE, TILE)
            weight = jnp.exp(r.cols[span, h : h + 1] - a_max)
            kw = weight * r.k[h, span, :].astype(F32)
            normal = normal + jnp.sum(kw, axis=0, keepdims=True)
            state = state + lax.dot_general(
                kw.astype(BF16),
                r.v[h, span, :],
                (((0,), (0,)), ((), ())),
                preferred_element_type=F32,
            )
        r.s_send[h] = state.reshape(quad, rows_own, HEAD_DIM).astype(BF16)
        r.a_send[h, 0:1, :] = jnp.broadcast_to(total + a_max, (1, HEAD_DIM))
        r.a_send[h, 1:2, :] = jnp.broadcast_to(total, (1, HEAD_DIM))
        r.a_send[h, 2:3, :] = normal
        r.a_send[h, 3:4, 0:part] = r.normal[h : h + 1, :]
        for step in range(1, n_sp):
            a_copy(h, step).start()
        for step in range(1, quad):
            s_copy(h, step).start()
        r.s_recv[h, my_slot] = r.s_send[h, my_slot]
        r.a_recv[sp, h] = r.a_send[h]

    def m_row(h, j):
        return pl.ds(h * (n_sp + 1) + j, 1)

    def chain(h):
        for step in range(1, n_sp):
            a_copy(h, step).wait()
        for j in range(n_sp):
            r.start[h : h + 1, j * part : (j + 1) * part] = r.a_recv[j, h, 3:4, 0:part]
        normal = r.start[h : h + 1, :]
        stab = jnp.zeros((1, HEAD_DIM), F32)
        my_stab, my_normal = stab, normal
        for j in range(n_sp):
            r.m[m_row(h, j), :] = stab
            if j > 0:
                my_stab = jnp.where(sp == j, stab, my_stab)
                my_normal = jnp.where(sp == j, normal, my_normal)
            late = r.a_recv[j, h, 0:1, :]
            keep = r.a_recv[j, h, 1:2, :]
            joint = jnp.maximum(late, keep + stab)
            normal = normal * jnp.exp(keep + stab - joint) + r.a_recv[j, h, 2:3, :] * jnp.exp(
                late - joint
            )
            stab = joint
        r.m[m_row(h, n_sp), :] = stab
        r.enter[h : h + 1, :] = my_stab
        r.enter[H + h : H + h + 1, :] = my_normal

    def spread(h):
        state = r.state[h]
        for i in range(quad):
            j = my_quad * quad + i
            r.e_send[h, i] = state.astype(BF16)
            stab, joint = r.m[m_row(h, j), :], r.m[m_row(h, j + 1), :]
            late = r.a_recv[j, h, 0:1, :]
            keep = r.a_recv[j, h, 1:2, :]
            state = state * jnp.exp(keep + stab - joint) + r.s_recv[h, i].astype(F32) * jnp.exp(
                late - joint
            )
        r.t_send[h] = state.astype(BF16)

        @pl.when(my_quad < quads - 1)
        def _():
            t_copy(h).start()

        for step in range(1, quad):
            e_copy(h, step).start()
        r.e_recv[h, my_slot] = r.e_send[h, my_slot]

    def gathered(h):
        chain(h)
        for step in range(1, quad):
            s_copy(h, step).wait()

        @pl.when(my_quad == 0)
        def _():
            if h == 0:
                for turn_in in range(per_owner):
                    source = sp * per_owner + turn_in

                    @pl.when(source != sp)
                    def _():
                        init_copy_from(turn_in).wait_recv()

                @pl.when(owner == sp)
                def _():
                    init_local.wait()

            r.state[h] = r.init[h]
            spread(h)

    def init_copy_from(turn_in):
        place = r.init.at[:, pl.ds(turn_in * part, part), :]
        return remote(init_hbm, place, r.init_sems.at[per_owner], r.init_sems.at[turn_in], "sp", owner)

    def carried_on(h):
        @pl.when(my_quad > 0)
        def _():
            t_copy(h).wait_recv()
            r.state[h] = r.t_recv[h].astype(F32)
            spread(h)

    loads["wq"].wait()

    def query_to(h):
        def store(rows, value):
            r.q[h, rows, :] = value.astype(BF16) * head_scale

        return store

    for h in range(H):
        product(r.wq, head_lanes(h), slice(0, T), query_to(h))
    gathered(0)
    loads["wpi"].wait()

    def store_pool(rows, value):
        r.ext[WIDEST + rows.start : WIDEST + rows.stop, :] = value.astype(BF16)

    for piece in range(2):
        product(r.wpi, slice(None), slice(piece * T // 2, (piece + 1) * T // 2), store_pool)
    halo = remote(
        r.ext.at[pl.ds(T, WIDEST)],
        r.ext.at[pl.ds(0, WIDEST)],
        r.halo_sems.at[0],
        r.halo_sems.at[1],
        "sp",
        lax.rem(sp + 1, n_sp),
    )
    for h in range(1, H):
        gathered(h)
    halo.start()

    for name in ("wg", "mem_gain", "wpg", "pool_gain", "mix"):
        loads[name].wait()
    chips = n_tp // 2
    chip, core = tp // 2, lax.rem(tp, 2)
    sibling = chip * 2 + 1 - core
    block = T // n_tp
    segment = 2 * block

    def gate_to(h):
        def store(rows, value):
            r.gate[h, rows, :] = r.mem_gain[:, head_lanes(h)] * silu(value)

        return store

    def store_gate(rows, value):
        r.pgate[rows, :] = r.pool_gain[...] * silu(value)

    def gates_of(target):
        start = pl.multiple_of(target * segment, segment)
        for h in range(H):
            product(r.wg, head_lanes(h), pl.ds(start, segment), gate_to(h))
        for piece in range(2):
            rows = pl.ds(pl.multiple_of(start + piece * block, block), block)
            product(r.wpg, slice(None), rows, store_gate)

    for j in range(1, chips):
        gates_of(lax.rem(chip + j, chips))
    carried_on(0)
    diag_mask = lax.broadcasted_iota(jnp.int32, (TILE, TILE), 0) >= lax.broadcasted_iota(
        jnp.int32, (TILE, TILE), 1
    )

    def attend(h):
        enter_max = r.enter[h : h + 1, 0:1]
        enter_normal = r.enter[H + h : H + h + 1, :]
        for t in range(tiles):
            span = pl.ds(t * TILE, TILE)
            queries = r.q[h, span, :]
            near = jnp.where(diag_mask, r.rows[h : h + 1, span], FLOOR)
            top = jnp.max(near, axis=-1, keepdims=True)
            if t > 0:
                far = r.rows[h : h + 1, 0 : t * TILE]
                top = jnp.maximum(top, jnp.max(far, axis=-1, keepdims=True))
            weights = jnp.exp(near - top) * dot_t(queries, r.k[h, span, :])
            den = jnp.sum(weights, axis=-1, keepdims=True)
            num = dot(weights.astype(BF16), r.v[h, span, :])
            if t > 0:
                weights = jnp.exp(far - top) * dot_t(queries, r.k[h, 0 : t * TILE, :])
                den = den + jnp.sum(weights, axis=-1, keepdims=True)
                num = num + dot(weights.astype(BF16), r.v[h, 0 : t * TILE, :])
            keep = r.cols[span, H + h : H + h + 1]
            row_max = keep + top
            carried = keep + enter_max
            joint = jnp.maximum(row_max, carried)
            local_weight = jnp.exp(row_max - joint)
            carry_weight = jnp.exp(carried - joint)
            den = den * local_weight + carry_weight * jnp.sum(
                queries.astype(F32) * enter_normal, axis=-1, keepdims=True
            )
            bound = jnp.maximum(jnp.abs(den), jnp.exp(-joint))
            r.num[h, span, :] = num * (local_weight / bound)
            r.beta[h, span, :] = carry_weight / bound

    attend(0)
    for h in range(1, H):
        carried_on(h)
    for h in range(1, H):
        attend(h)
    halo.wait()

    def pool_of(target):
        for g in range(G):
            window = jnp.left_shift(2, tp * G + g)
            offset = (
                lax.broadcasted_iota(jnp.int32, (TILE, TILE + WIDEST), 0)
                + WIDEST
                - lax.broadcasted_iota(jnp.int32, (TILE, TILE + WIDEST), 1)
            )
            band = jnp.where((offset >= 0) & (offset < window), 1.0, 0.0).astype(BF16)
            lanes = slice(g * GROUP_DIM, (g + 1) * GROUP_DIM)
            for piece in range(segment // TILE):
                start = pl.multiple_of(target * segment + piece * TILE, TILE)
                span = pl.ds(start, TILE)
                here = r.ext[pl.ds(pl.multiple_of(start + WIDEST, TILE), TILE), lanes]
                before = r.ext[pl.ds(start, WIDEST), lanes]
                before = jnp.where(sp + start > 0, before.astype(F32), 0.0).astype(BF16)
                sums = dot(band[:, :WIDEST], before) + dot(band[:, WIDEST:], here)
                position = lax.broadcasted_iota(jnp.int32, (TILE, 1), 0) + (sp * T + start + 1)
                counts = jnp.minimum(position, window).astype(F32)
                pooled = (sums / counts - here.astype(F32)).astype(BF16)
                r.pool[span, lanes] = (dot(pooled, r.mix[g]) * r.pgate[span, lanes]).astype(BF16)

    for j in range(1, chips):
        pool_of(lax.rem(chip + j, chips))
    loads["wop"].wait()
    loads["wom"].wait()
    loads["post"].wait()
    size = block // CHUNKS
    slots = chips * CHUNKS

    def chunk_rows(target, which, n):
        return pl.ds(pl.multiple_of((target * 2 + which) * block + n * size, size), size)

    def memory_product(rows):
        parts = [(r.num[h, rows, :] * r.gate[h, rows, :]).astype(BF16) for h in range(H)]
        return dot(parts[0] if H == 1 else jnp.concatenate(parts, axis=1), r.wom[...])

    def finish(rows):
        pool = dot(r.pool[rows, :], r.wop[...])
        return (memory_product(rows) * r.scale[rows, 0:1] + pool).astype(BF16)

    jobs = []
    for j in range(1, chips + 1):
        for n in range(CHUNKS):
            jobs.append((j, n, lax.rem(chip + j, chips), (j - 1) * CHUNKS + n))

    siblings, links = {}, {}

    def to_sibling(slot):
        siblings[slot] = remote(
            r.sib_send.at[slot],
            r.sib_recv.at[slot],
            r.sib_sems.at[0, slot],
            r.sib_sems.at[1, slot],
            "tp",
            sibling,
        )
        siblings[slot].start()

    def to_chip(slot, target):
        links[slot] = remote(
            r.link_send.at[slot],
            r.link_recv.at[slot],
            r.link_sems.at[0, slot],
            r.link_sems.at[1, slot],
            "tp",
            target * 2 + core,
        )
        links[slot].start()

    lead_theirs = chunk_rows(jobs[0][2], 1 - core, 0)
    lead_ours = chunk_rows(jobs[0][2], core, 0)
    r.sib_send[slots] = dot(r.pool[lead_theirs, :], r.wop[...]).astype(BF16)
    to_sibling(slots)
    r.lead_pool[...] = dot(r.pool[lead_ours, :], r.wop[...])

    def piece_spans(n):
        return [slice(b * block + n * size, b * block + (n + 1) * size) for b in range(n_tp)]

    def combine(h, n):
        spans = piece_spans(n)
        state = r.e_recv[h].reshape(HEAD_DIM, HEAD_DIM)
        carried = dot(jnp.concatenate([r.q[h, span, :] for span in spans], axis=0), state)
        squares = []
        for b, span in enumerate(spans):
            memory = r.num[h, span, :] + r.beta[h, span, :] * carried[b * size : (b + 1) * size]
            r.num[h, span, :] = memory
            squares.append(jnp.sum(memory * memory, axis=-1, keepdims=True))
        squares = jnp.concatenate(squares, axis=0)
        if h > 0:
            squares = squares + jnp.concatenate([r.squares[span] for span in spans], axis=0)
        r.sq_send[n] = jnp.broadcast_to(squares, (n_tp * size, 128)).T[0:1]

    def combine_early(h):
        state = r.e_recv[h].reshape(HEAD_DIM, HEAD_DIM)
        for t in range(tiles):
            span = slice(t * TILE, (t + 1) * TILE)
            carried = dot(r.q[h, span, :], state)
            memory = r.num[h, span, :] + r.beta[h, span, :] * carried
            r.num[h, span, :] = memory
            squares = jnp.sum(memory * memory, axis=-1, keepdims=True)
            if h > 0:
                squares = squares + r.squares[span]
            r.squares[span] = squares

    def square_copies(which):
        pieces = slice(0, 1) if which == 0 else slice(1, CHUNKS)
        made = []
        for step in range(1, n_tp):
            made.append(
                remote(
                    r.sq_send.at[pieces],
                    r.sq_recv.at[step, pieces],
                    r.sq_sems.at[0, which, step],
                    r.sq_sems.at[1, which, step],
                    "tp",
                    lax.rem(tp + step, n_tp),
                )
            )
        return made

    def scales(pieces):
        for n in pieces:
            total = r.sq_send[n]
            for step in range(1, n_tp):
                total = total + r.sq_recv[step, n]
            scale = lax.rsqrt(total / (HEAD_DIM * H * n_tp) + EPS)
            scale = jnp.broadcast_to(scale, (128, n_tp * size)).T
            for b, span in enumerate(piece_spans(n)):
                r.scale[span, :] = scale[b * size : (b + 1) * size]

    for h in range(H):
        for step in range(1, quad):
            e_copy(h, step).wait()
        if h < H - 1:
            combine_early(h)
    lead_squares, rest_squares = square_copies(0), square_copies(1)
    combine(H - 1, 0)
    for copy in lead_squares:
        copy.start()
    r.sib_send[0] = memory_product(lead_theirs).astype(BF16)
    to_sibling(0)
    for n in range(1, CHUNKS):
        combine(H - 1, n)
    for copy in rest_squares:
        copy.start()
    r.lead_memory[...] = memory_product(lead_ours)
    for copy in lead_squares:
        copy.wait()
    scales([0])

    siblings[slots].wait_recv()
    siblings[0].wait_recv()
    r.link_send[0] = (
        (r.lead_memory[...] + r.sib_recv[0].astype(F32)) * r.scale[lead_ours, 0:1]
        + r.lead_pool[...]
        + r.sib_recv[slots].astype(F32)
    ).astype(BF16)
    to_chip(0, jobs[0][2])

    def send_on(job):
        j, n, target, slot = job
        if j == chips:
            return
        siblings[slot].wait_recv()
        r.link_send[slot] = (r.own[slot].astype(F32) + r.sib_recv[slot].astype(F32)).astype(BF16)
        to_chip(slot, target)

    for copy in rest_squares:
        copy.wait()
    scales(range(1, CHUNKS))
    for index, (j, n, target, slot) in enumerate(jobs):
        if index == 0:
            continue
        if j == chips and n == 0:
            gates_of(chip)
            pool_of(chip)
        r.sib_send[slot] = finish(chunk_rows(target, 1 - core, n))
        to_sibling(slot)
        r.own[slot] = finish(chunk_rows(target, core, n))
        if index > 1:
            send_on(jobs[index - 1])
    outs = []
    for n in range(CHUNKS):
        slot = (chips - 1) * CHUNKS + n
        siblings[slot].wait_recv()
        total = r.own[slot].astype(F32) + r.sib_recv[slot].astype(F32)
        for j in range(1, chips):
            other = (j - 1) * CHUNKS + n
            links[other].wait_recv()
            total = total + r.link_recv[other].astype(F32)
        scale = lax.rsqrt(jnp.mean(total * total, axis=-1, keepdims=True) + EPS)
        span = pl.ds(n * size, size)
        out_hbm[span, :] = (total * scale * r.post[...]).astype(BF16)

    @pl.when(owner != sp)
    def _():
        init_copy.wait_send()

    for h in range(H):
        @pl.when(my_quad < quads - 1)
        def _(h=h):
            t_copy(h).wait_send()

    for copy in [*siblings.values(), *links.values()]:
        copy.wait_send()
    for copy in outs:
        copy.wait()


def body(
    n_sp,
    n_tp,
    tokens,
    pre_gain,
    w_query,
    w_key,
    w_value,
    memory_output_gate_weight,
    w_input_gate,
    w_forget_gate,
    input_bias,
    forget_bias,
    forget_extra,
    initial_memory,
    initial_normal,
    memory_gain,
    w_pool_input,
    w_pool_gate,
    pool_mix,
    pool_gain,
    w_out_memory,
    w_out_pool,
    post_gain,
):
    T, D = tokens.shape
    MW = w_query.shape[1]
    PW = w_pool_input.shape[1]
    H = MW // HEAD_DIM
    G = PW // GROUP_DIM
    heads = w_input_gate.shape[1]
    part = initial_normal.shape[1]
    quad = min(QUAD, n_sp)
    rows_own = HEAD_DIM // quad
    chips = n_tp // 2
    block = T // n_tp
    slots = chips * CHUNKS
    size = block // CHUNKS
    hbm = pl.BlockSpec(memory_space=pl.ANY)
    V = pltpu.VMEM
    dma = pltpu.SemaphoreType.DMA
    scratch = dict(
        tokens=V((T, D), BF16),
        gain=V((1, D), F32),
        wq=V((D, MW), BF16),
        wk=V((D, MW), BF16),
        wv=V((D, MW), BF16),
        wg=V((D, MW), BF16),
        w_in=V((heads, D), BF16),
        w_forget=V((heads, D), BF16),
        b_in=V((1, heads), F32),
        b_forget=V((1, heads), F32),
        extra=V((H, T), F32),
        normal=V((H, part), F32),
        mem_gain=V((1, MW), F32),
        wpi=V((D, PW), BF16),
        wpg=V((D, PW), BF16),
        mix=V((G, GROUP_DIM, GROUP_DIM), BF16),
        pool_gain=V((1, PW), F32),
        wom=V((MW, D), BF16),
        wop=V((PW, D), BF16),
        post=V((1, D), F32),
        normed=V((T, D), BF16),
        q=V((H, T, HEAD_DIM), BF16),
        k=V((H, T, HEAD_DIM), BF16),
        v=V((H, T, HEAD_DIM), BF16),
        gate=V((H, T, HEAD_DIM), F32),
        pgate=V((T, PW), F32),
        ext=V((T + WIDEST, PW), BF16),
        pool=V((T, PW), BF16),
        rows=V((128, T), F32),
        cols=V((T, 128), F32),
        num=V((H, T, HEAD_DIM), F32),
        beta=V((H, T, 1), F32),
        gates_w=V((128, D), BF16),
        gates_b=V((1, 128), F32),
        raw=V((128, T), F32),
        start=V((8, HEAD_DIM), F32),
        enter=V((2 * H, HEAD_DIM), F32),
        m=V((H * (n_sp + 1), HEAD_DIM), F32),
        init=V((H, rows_own, HEAD_DIM), F32),
        state=V((H, rows_own, HEAD_DIM), F32),
        a_send=V((H, 4, HEAD_DIM), F32),
        a_recv=V((n_sp, H, 4, HEAD_DIM), F32),
        s_send=V((H, quad, rows_own, HEAD_DIM), BF16),
        s_recv=V((H, quad, rows_own, HEAD_DIM), BF16),
        e_send=V((H, quad, rows_own, HEAD_DIM), BF16),
        e_recv=V((H, quad, rows_own, HEAD_DIM), BF16),
        t_send=V((H, rows_own, HEAD_DIM), BF16),
        t_recv=V((H, rows_own, HEAD_DIM), BF16),
        squares=V((T, 1), F32),
        sq_send=V((CHUNKS, 1, T // CHUNKS), F32),
        sq_recv=V((n_tp, CHUNKS, 1, T // CHUNKS), F32),
        lead_pool=V((size, D), F32),
        lead_memory=V((size, D), F32),
        scale=V((T, 128), F32),
        sib_send=V((slots + 1, size, D), BF16),
        sib_recv=V((slots + 1, size, D), BF16),
        own=V((slots, size, D), BF16),
        link_send=V((slots, size, D), BF16),
        link_recv=V((slots, size, D), BF16),
        local_sem=dma((INPUTS + T // TILE + 2 * H,)),
        init_sems=dma((n_sp // quad + 1,)),
        a_sems=dma((2, H, n_sp)),
        s_sems=dma((2, H, quad)),
        e_sems=dma((2, H, quad)),
        t_sems=dma((2, H)),
        halo_sems=dma((2,)),
        sq_sems=dma((2, 2, n_tp)),
        sib_sems=dma((2, slots + 1)),
        link_sems=dma((2, slots)),
    )
    return pl.pallas_call(
        functools.partial(kernel, n_sp, n_tp, tuple(scratch)),
        out_shape=pltpu.VMEM((block, D), BF16),
        in_specs=[hbm] * INPUTS,
        out_specs=pl.BlockSpec(memory_space=pltpu.VMEM),
        scratch_shapes=list(scratch.values()),
        compiler_params=pltpu.CompilerParams(
            collective_id=0, has_side_effects=True, vmem_limit_bytes=60 * 1024 * 1024
        ),
    )(
        tokens,
        pre_gain[None],
        w_query,
        w_key,
        w_value,
        memory_output_gate_weight,
        w_input_gate.T,
        w_forget_gate.T,
        input_bias[None],
        forget_bias[None],
        forget_extra.T,
        initial_memory,
        initial_normal,
        memory_gain[None],
        w_pool_input,
        w_pool_gate,
        pool_mix,
        pool_gain[None],
        w_out_memory,
        w_out_pool,
        post_gain[None],
    )


def solution(mesh):
    in_specs = (
        P("sp", None),
        P(),
        P(None, "tp"),
        P(None, "tp"),
        P(None, "tp"),
        P(None, "tp"),
        P(),
        P(),
        P(),
        P(),
        P("sp", "tp"),
        P("tp", "sp", None),
        P("tp", "sp"),
        P(),
        P(None, "tp"),
        P(None, "tp"),
        P(),
        P(),
        P("tp", None),
        P("tp", None),
        P(),
    )
    out_specs = P(("sp", "tp"), None)
    sizes = dict(mesh.shape)
    run = functools.partial(body, sizes["sp"], sizes["tp"])
    return jax.shard_map(run, mesh=mesh, in_specs=in_specs, out_specs=out_specs, check_vma=False)
```

time: 79.5 us -> 57.7 us (0.73); the launches traced: 78.5 us -> 57.5 us
  Pallas kernels: 70.9 us -> 56.5 us
  local copies, waits for them, and re-layouts: 7.58 us -> 0.97 us
    pallas_call x1, Pallas kernels: 70.9 us -> 56.5 us  [body(): pl.pallas_call(functools.partial(kernel, n_sp, n_tp, tuple(scratch)), out...]
    unnamed x4 -> x1, local copies, waits for them, and re-layouts: 7.58 us -> 0.97 us
where the time goes in v1:
time: 57.7 us; the launch traced here: 57.5 us
  Pallas kernels  56.5 us (98%)
  local copies, waits for them, and re-layouts  0.97 us (2%)
    pallas_call x1, Pallas kernels, body(): pl.pallas_call(functools.partial(kernel, n_sp, n_tp, tuple(scratch)), out...  56.5 us

profile of v1, /device:TPU:0, one launch (start us, length us, event | category | flops | bytes accessed | tf_op | source)
XLA Modules:
  0.0 57.5 jit_solution(14321724310786757875)
XLA Ops:
  0.0 56.5 %shard_map.199 = bf16[256,2048]{1,0:T(8,128)(2,1)S(1)} custom-call(bf16[1024,2048]{1,0:T(8,128)(2,1)} %refs_0_.1, f32[1,2048]{1,0:T(1,128)} %bitcast.11, bf16[2048,512]{1,0:T(8,128)(2,1)} %refs_2_.1, bf16[2048,512]{1,0:T(8,128)(2,1)} %refs_3_.1, bf16[2048,512]{1,0:T(8,128)(2,1)} %refs_4_.1, bf16[2048,512]{1,0:T(8,128)(2,1)} %refs_5_.1, ...), custom_call_target="tpu_custom_call" | custom-call | tf_op jit(solution)/shard_map/pallas_call | solution.py:817
  56.5 1.0 %copy.23 = bf16[256,2048]{1,0:T(8,128)(2,1)} copy(bf16[256,2048]{1,0:T(8,128)(2,1)S(1)} %shard_map.199) | data formatting | bytes 2097152

commit v2 on v1

--- a/solution.py
+++ b/solution.py
@@ -12,7 +12,7 @@
 GROUP_DIM = 128
 WIDEST = 256
 TILE = 256
-CHUNKS = 4
+SHARES = (2, 1, 1, 2, 2)
 QUAD = 4
 SUB = 64
 EPS = 1e-06
@@ -59,7 +59,7 @@
         wop_hbm,
         post_hbm,
     ) = refs[:INPUTS]
-    out_hbm = refs[INPUTS]
+    out_ref = refs[INPUTS]
     r = types.SimpleNamespace(**dict(zip(names, refs[INPUTS + 1 :])))
     T, D = r.tokens.shape
     H = r.q.shape[0]
@@ -79,8 +79,9 @@
     pool_lanes = pl.ds(pl.multiple_of(tp * G * GROUP_DIM, GROUP_DIM), G * GROUP_DIM)
     loads = {}
 
-    def load(name, src, dst):
-        loads[name] = pltpu.make_async_copy(src, dst, r.local_sem.at[len(loads)])
+    def load(name, src, dst, slot=None):
+        slot = len(loads) if slot is None else slot
+        loads[name] = pltpu.make_async_copy(src, dst, r.local_sem.at[slot])
         loads[name].start()
 
     load("gain", gain_hbm, r.gain)
@@ -110,15 +111,8 @@
         load_head("wv", wv_hbm, r.wv, h)
     load("wpi", wpi_hbm, r.wpi)
     load("wq", wq_hbm, r.wq)
-    load("wpg", wpg_hbm, r.wpg)
-    load("wg", wg_hbm, r.wg)
-    load("mix", mix_hbm.at[pl.ds(tp * G, G)], r.mix)
-    load("pool_gain", pool_gain_hbm.at[:, pool_lanes], r.pool_gain)
-    load("mem_gain", mem_gain_hbm.at[:, mem_lanes], r.mem_gain)
-    load("wop", wop_hbm, r.wop)
-    load("wom", wom_hbm, r.wom)
-    load("post", post_hbm, r.post)
-
+
+    r.ext[0:WIDEST, :] = jnp.zeros((WIDEST, r.ext.shape[1]), BF16)
     barrier = pltpu.get_barrier_semaphore()
     for step in range(1, n_sp):
         pl.semaphore_signal(
@@ -191,47 +185,70 @@
             norm_tile(pl.ds(t * TILE + sub, SUB))
     for name in ("w_in", "w_forget", "b_in", "b_forget", ("wk", 0)):
         loads[name].wait()
+    load("wpg", wpg_hbm, r.wpg, 0)
+    load("wg", wg_hbm, r.wg, 1)
+    load("mix", mix_hbm.at[pl.ds(tp * G, G)], r.mix, 2)
+    load("pool_gain", pool_gain_hbm.at[:, pool_lanes], r.pool_gain, 3)
+    load("mem_gain", mem_gain_hbm.at[:, mem_lanes], r.mem_gain, 4)
+    load("wop", wop_hbm, r.wop, 5)
+    load("wom", wom_hbm, r.wom, 6)
+    load("post", post_hbm, r.post, 7)
     r.gates_w[0:heads, :] = r.w_in[...]
     r.gates_w[heads : 2 * heads, :] = r.w_forget[...]
     r.gates_b[:, 0:heads] = r.b_in[...]
     r.gates_b[:, heads : 2 * heads] = r.b_forget[...]
-    for t in range(half, tiles):
-        loads["tokens", t].wait()
-
     def early_products(rows):
         gates_product(rows)
         product(r.wk, head_lanes(0), rows, whole(r.k, 0))
 
     pieces = (slice(0, half * TILE), slice(half * TILE, T))
+    loads["tokens", half].wait()
     early_products(pieces[0])
     for t in range(half, tiles):
+        if t > half:
+            loads["tokens", t].wait()
+            if t == half + 1:
+                loads["wv", 0].wait()
+                for part_rows in (slice(0, TILE), slice(TILE, half * TILE)):
+                    product(r.wv, head_lanes(0), part_rows, whole(r.v, 0))
         for sub in range(0, TILE, SUB):
             norm_tile(pl.ds(t * TILE + sub, SUB))
-    for name in (("wv", 0), "extra", "normal"):
+    send_init()
+    for name in ("extra", "normal"):
         loads[name].wait()
+    for h in range(1, H):
+        loads["wk", h].wait()
+        loads["wv", h].wait()
     early_products(pieces[1])
-    send_init()
-    for rows in pieces:
-        product(r.wv, head_lanes(0), rows, whole(r.v, 0))
+    for start in (half * TILE, half * TILE + TILE):
+        product(r.wv, head_lanes(0), slice(start, start + TILE), whole(r.v, 0))
 
     tri = (
         lax.broadcasted_iota(jnp.int32, (TILE, TILE), 0)
         <= lax.broadcasted_iota(jnp.int32, (TILE, TILE), 1)
     ).astype(F32)
-    carry = jnp.zeros((8, 1), F32)
+    spare = [jnp.zeros((8 - H, TILE), F32)]
+    log_keeps = []
     for t in range(tiles):
         span = pl.ds(t * TILE, TILE)
         r.raw[:, span] = r.cols[span, :].T
         own_rows = [r.raw[pl.ds(heads + tp * H + h, 1), span] for h in range(H)]
         added = [r.extra[h : h + 1, span] for h in range(H)]
-        spare = [jnp.zeros((8 - H, TILE), F32)]
         raw = jnp.concatenate(own_rows + spare, axis=0)
         log_keep = jnp.minimum(raw, 0.0) - jnp.log1p(jnp.exp(-jnp.abs(raw)))
-        log_keep = log_keep + jnp.concatenate(added + spare, axis=0)
-        run = carry + jnp.dot(
-            log_keep, tri, preferred_element_type=F32, precision=lax.Precision.HIGHEST
-        )
-        carry = run[:, TILE - 1 : TILE]
+        log_keeps.append(log_keep + jnp.concatenate(added + spare, axis=0))
+    runs = jnp.dot(
+        jnp.concatenate(log_keeps, axis=0),
+        tri,
+        preferred_element_type=F32,
+        precision=lax.Precision.HIGHEST,
+    )
+    last = [runs[8 * t : 8 * t + 8, TILE - 1 : TILE] for t in range(tiles)]
+    carry = jnp.zeros((8, 1), F32)
+    for t in range(tiles):
+        span = pl.ds(t * TILE, TILE)
+        run = carry + runs[8 * t : 8 * t + 8]
+        carry = carry + last[t]
         for h in range(H):
             keep = run[h : h + 1]
             r.rows[h : h + 1, span] = r.raw[pl.ds(tp * H + h, 1), span] - keep
@@ -243,7 +260,7 @@
     def a_copy(h, step):
         peer = lax.rem(sp + step, n_sp)
         return remote(
-            r.a_send.at[h], r.a_recv.at[sp, h], r.a_sems.at[0, h, step], r.a_sems.at[1, h, step], "sp", peer
+            r.a_send.at[h], r.a_recv.at[sp, h], r.a_sems.at[0, h], r.a_sems.at[1, h], "sp", peer
         )
 
     def s_copy(h, step):
@@ -251,8 +268,8 @@
         return remote(
             r.s_send.at[h, peer],
             r.s_recv.at[h, my_slot],
-            r.s_sems.at[0, h, step],
-            r.s_sems.at[1, h, step],
+            r.s_sems.at[0, h],
+            r.s_sems.at[1, h],
             "sp",
             my_quad * quad + peer,
         )
@@ -262,11 +279,15 @@
         return remote(
             r.e_send.at[h, peer],
             r.e_recv.at[h, my_slot],
-            r.e_sems.at[0, h, step],
-            r.e_sems.at[1, h, step],
+            r.e_sems.at[0, h],
+            r.e_sems.at[1, h],
             "sp",
             my_quad * quad + peer,
         )
+
+    def all_of(ref, sems, axis="sp"):
+        peer = lax.rem(sp + 1, n_sp) if axis == "sp" else lax.rem(tp + 1, n_tp)
+        return remote(ref, ref, sems[0], sems[1], axis, peer)
 
     def t_copy(h):
         return remote(
@@ -280,10 +301,10 @@
 
     for h in range(H):
         if h > 0:
-            loads["wk", h].wait()
-            loads["wv", h].wait()
-            product(r.wk, head_lanes(h), slice(0, T), whole(r.k, h))
-            product(r.wv, head_lanes(h), slice(0, T), whole(r.v, h))
+            for rows in pieces:
+                product(r.wk, head_lanes(h), rows, whole(r.k, h))
+            for rows in pieces:
+                product(r.wv, head_lanes(h), rows, whole(r.v, h))
         a_max = jnp.max(r.rows[h : h + 1, :], axis=-1, keepdims=True)
         total = r.rows[H + h : H + h + 1, T - 1 : T]
         state = jnp.zeros((HEAD_DIM, HEAD_DIM), F32)
@@ -315,8 +336,7 @@
         return pl.ds(h * (n_sp + 1) + j, 1)
 
     def chain(h):
-        for step in range(1, n_sp):
-            a_copy(h, step).wait()
+        all_of(r.a_recv.at[pl.ds(0, n_sp - 1), h], (r.a_sems.at[0, h], r.a_sems.at[1, h])).wait()
         for j in range(n_sp):
             r.start[h : h + 1, j * part : (j + 1) * part] = r.a_recv[j, h, 3:4, 0:part]
         normal = r.start[h : h + 1, :]
@@ -361,8 +381,7 @@
 
     def gathered(h):
         chain(h)
-        for step in range(1, quad):
-            s_copy(h, step).wait()
+        all_of(r.s_recv.at[h, pl.ds(0, quad - 1)], (r.s_sems.at[0, h], r.s_sems.at[1, h])).wait()
 
         @pl.when(my_quad == 0)
         def _():
@@ -392,7 +411,32 @@
             r.state[h] = r.t_recv[h].astype(F32)
             spread(h)
 
+    loads["wpi"].wait()
     loads["wq"].wait()
+
+    def store_pool(rows, value):
+        r.ext[WIDEST + rows.start : WIDEST + rows.stop, :] = value.astype(BF16)
+
+    for rows in pieces:
+        product(r.wpi, slice(None), rows, store_pool)
+
+    def halo_copy(member):
+        width = min(WIDEST, max(16, 2 ** (G * (member + 1))))
+        return remote(
+            r.ext.at[pl.ds(T + WIDEST - width, width)],
+            r.ext.at[pl.ds(WIDEST - width, width)],
+            r.halo_sems.at[0],
+            r.halo_sems.at[1],
+            "sp",
+            lax.rem(sp + 1, n_sp),
+        )
+
+    for member in range(n_tp):
+
+        @pl.when((tp == member) & (sp < n_sp - 1))
+        def _(member=member):
+            halo_copy(member).start()
+
 
     def query_to(h):
         def store(rows, value):
@@ -400,35 +444,35 @@
 
         return store
 
-    for h in range(H):
-        product(r.wq, head_lanes(h), slice(0, T), query_to(h))
+    for rows in pieces:
+        product(r.wq, head_lanes(0), rows, query_to(0))
     gathered(0)
-    loads["wpi"].wait()
-
-    def store_pool(rows, value):
-        r.ext[WIDEST + rows.start : WIDEST + rows.stop, :] = value.astype(BF16)
-
-    for piece in range(2):
-        product(r.wpi, slice(None), slice(piece * T // 2, (piece + 1) * T // 2), store_pool)
-    halo = remote(
-        r.ext.at[pl.ds(T, WIDEST)],
-        r.ext.at[pl.ds(0, WIDEST)],
-        r.halo_sems.at[0],
-        r.halo_sems.at[1],
-        "sp",
-        lax.rem(sp + 1, n_sp),
-    )
     for h in range(1, H):
-        gathered(h)
-    halo.start()
-
-    for name in ("wg", "mem_gain", "wpg", "pool_gain", "mix"):
+        for rows in pieces:
+            product(r.wq, head_lanes(h), rows, query_to(h))
+    for name in ("wg", "mem_gain", "wpg", "pool_gain", "mix", "wop", "wom", "post"):
         loads[name].wait()
     chips = n_tp // 2
     chip, core = tp // 2, lax.rem(tp, 2)
     sibling = chip * 2 + 1 - core
     block = T // n_tp
     segment = 2 * block
+    unit = block // sum(SHARES)
+    chunks = []
+    for share in SHARES:
+        begin = chunks[-1][0] + chunks[-1][1] if chunks else 0
+        chunks.append((begin, share * unit))
+    count = len(chunks)
+    extra_slot = chips * count
+    lead = chunks[0][1]
+
+    def chunk_rows(target, which, n):
+        begin, size = chunks[n]
+        return pl.ds(pl.multiple_of((target * 2 + which) * block + begin, unit), size)
+
+    first_target = lax.rem(chip + 1, chips)
+    lead_theirs = chunk_rows(first_target, 1 - core, 0)
+    lead_ours = chunk_rows(first_target, core, 0)
 
     def gate_to(h):
         def store(rows, value):
@@ -447,8 +491,107 @@
             rows = pl.ds(pl.multiple_of(start + piece * block, block), block)
             product(r.wpg, slice(None), rows, store_gate)
 
-    for j in range(1, chips):
-        gates_of(lax.rem(chip + j, chips))
+    def lead_pair(ref):
+        return jnp.concatenate([ref[lead_theirs, :], ref[lead_ours, :]], axis=0)
+
+    def pool_rows(start, size):
+        for g in range(G):
+            window = jnp.left_shift(2, tp * G + g)
+            offset = (
+                lax.broadcasted_iota(jnp.int32, (size, size + WIDEST), 0)
+                + WIDEST
+                - lax.broadcasted_iota(jnp.int32, (size, size + WIDEST), 1)
+            )
+            band = jnp.where((offset >= 0) & (offset < window), 1.0, 0.0).astype(BF16)
+            lanes = slice(g * GROUP_DIM, (g + 1) * GROUP_DIM)
+            span = pl.ds(start, size)
+            here = r.ext[pl.ds(pl.multiple_of(start + WIDEST, unit), size), lanes]
+            before = r.ext[pl.ds(start, WIDEST), lanes]
+            sums = dot(band[:, :WIDEST], before) + dot(band[:, WIDEST:], here)
+            position = lax.broadcasted_iota(jnp.int32, (size, 1), 0) + (sp * T + start + 1)
+            counts = jnp.minimum(position, window).astype(F32)
+            pooled = (sums / counts - here.astype(F32)).astype(BF16)
+            r.pool[span, lanes] = (dot(pooled, r.mix[g]) * r.pgate[span, lanes]).astype(BF16)
+
+    def pool_of(target):
+        for piece in range(segment // TILE):
+            pool_rows(pl.multiple_of(target * segment + piece * TILE, TILE), TILE)
+
+    value = dot(lead_pair(r.normed), r.wpg[...])
+    store_gate(lead_theirs, value[:lead])
+    store_gate(lead_ours, value[lead:])
+    value = dot(lead_pair(r.normed), r.wg[...])
+    for h in range(H):
+        gate_to(h)(lead_theirs, value[:lead, head_lanes(h)])
+        gate_to(h)(lead_ours, value[lead:, head_lanes(h)])
+    for h in range(1, H):
+        gathered(h)
+    for member in range(n_tp):
+
+        @pl.when((tp == member) & (sp > 0))
+        def _(member=member):
+            halo_copy(member).wait_recv()
+
+    for which in (1 - core, core):
+        pool_rows(pl.multiple_of((first_target * 2 + which) * block, block), lead)
+    def memory_product(rows):
+        parts = [(r.num[h, rows, :] * r.gate[h, rows, :]).astype(BF16) for h in range(H)]
+        return dot(parts[0] if H == 1 else jnp.concatenate(parts, axis=1), r.wom[...])
+
+    def finish(rows):
+        pool = dot(r.pool[rows, :], r.wop[...])
+        return (memory_product(rows) * r.scale[rows, 0:1] + pool).astype(BF16)
+
+    jobs = []
+    for j in range(1, chips + 1):
+        for n in range(count):
+            jobs.append((j, n, lax.rem(chip + j, chips)))
+
+    siblings, links = {}, {}
+
+    def place(j, n):
+        if n < 0:
+            return pl.ds(chips * block, lead)
+        begin, size = chunks[n]
+        return pl.ds((j - 1) * block + begin, size)
+
+    def to_sibling(j, n):
+        slot = extra_slot if n < 0 else (j - 1) * count + n
+        rows = place(j, n)
+        siblings[j, n] = remote(
+            r.sib_send.at[rows],
+            r.sib_recv.at[rows],
+            r.sib_sems.at[extra_slot + 1],
+            r.sib_sems.at[slot],
+            "tp",
+            sibling,
+        )
+        siblings[j, n].start()
+
+    def to_chip(j, n, target):
+        slot = extra_slot - count if n < 0 else (j - 1) * count + n
+        rows = place(j, n)
+        links[j, n] = remote(
+            r.link_send.at[rows],
+            r.link_recv.at[rows],
+            r.link_sems.at[extra_slot - count + 1],
+            r.link_sems.at[slot],
+            "tp",
+            target * 2 + core,
+        )
+        links[j, n].start()
+
+    r.sib_send[place(1, -1), :] = dot(r.pool[lead_theirs, :], r.wop[...]).astype(BF16)
+    to_sibling(1, -1)
+    r.lead[...] = dot(r.pool[lead_ours, :], r.wop[...])
+
+    def pass_on(j, n, target):
+        siblings[j, n].wait_recv()
+        rows = place(j, n)
+        mine = r.lead[...] if (j, max(n, 0)) == (1, 0) else r.own[rows, :].astype(F32)
+        r.link_send[rows, :] = (mine + r.sib_recv[rows, :].astype(F32)).astype(BF16)
+        to_chip(j, n, target)
+
     carried_on(0)
     diag_mask = lax.broadcasted_iota(jnp.int32, (TILE, TILE), 0) >= lax.broadcasted_iota(
         jnp.int32, (TILE, TILE), 1
@@ -486,106 +629,13 @@
             r.beta[h, span, :] = carry_weight / bound
 
     attend(0)
+    pass_on(1, -1, first_target)
     for h in range(1, H):
         carried_on(h)
+
     for h in range(1, H):
         attend(h)
-    halo.wait()
-
-    def pool_of(target):
-        for g in range(G):
-            window = jnp.left_shift(2, tp * G + g)
-            offset = (
-                lax.broadcasted_iota(jnp.int32, (TILE, TILE + WIDEST), 0)
-                + WIDEST
-                - lax.broadcasted_iota(jnp.int32, (TILE, TILE + WIDEST), 1)
-            )
-            band = jnp.where((offset >= 0) & (offset < window), 1.0, 0.0).astype(BF16)
-            lanes = slice(g * GROUP_DIM, (g + 1) * GROUP_DIM)
-            for piece in range(segment // TILE):
-                start = pl.multiple_of(target * segment + piece * TILE, TILE)
-                span = pl.ds(start, TILE)
-                here = r.ext[pl.ds(pl.multiple_of(start + WIDEST, TILE), TILE), lanes]
-                before = r.ext[pl.ds(start, WIDEST), lanes]
-                before = jnp.where(sp + start > 0, before.astype(F32), 0.0).astype(BF16)
-                sums = dot(band[:, :WIDEST], before) + dot(band[:, WIDEST:], here)
-                position = lax.broadcasted_iota(jnp.int32, (TILE, 1), 0) + (sp * T + start + 1)
-                counts = jnp.minimum(position, window).astype(F32)
-                pooled = (sums / counts - here.astype(F32)).astype(BF16)
-                r.pool[span, lanes] = (dot(pooled, r.mix[g]) * r.pgate[span, lanes]).astype(BF16)
-
-    for j in range(1, chips):
-        pool_of(lax.rem(chip + j, chips))
-    loads["wop"].wait()
-    loads["wom"].wait()
-    loads["post"].wait()
-    size = block // CHUNKS
-    slots = chips * CHUNKS
-
-    def chunk_rows(target, which, n):
-        return pl.ds(pl.multiple_of((target * 2 + which) * block + n * size, size), size)
-
-    def memory_product(rows):
-        parts = [(r.num[h, rows, :] * r.gate[h, rows, :]).astype(BF16) for h in range(H)]
-        return dot(parts[0] if H == 1 else jnp.concatenate(parts, axis=1), r.wom[...])
-
-    def finish(rows):
-        pool = dot(r.pool[rows, :], r.wop[...])
-        return (memory_product(rows) * r.scale[rows, 0:1] + pool).astype(BF16)
-
-    jobs = []
-    for j in range(1, chips + 1):
-        for n in range(CHUNKS):
-            jobs.append((j, n, lax.rem(chip + j, chips), (j - 1) * CHUNKS + n))
-
-    siblings, links = {}, {}
-
-    def to_sibling(slot):
-        siblings[slot] = remote(
-            r.sib_send.at[slot],
-            r.sib_recv.at[slot],
-            r.sib_sems.at[0, slot],
-            r.sib_sems.at[1, slot],
-            "tp",
-            sibling,
-        )
-        siblings[slot].start()
-
-    def to_chip(slot, target):
-        links[slot] = remote(
-            r.link_send.at[slot],
-            r.link_recv.at[slot],
-            r.link_sems.at[0, slot],
-            r.link_sems.at[1, slot],
-            "tp",
-            target * 2 + core,
-        )
-        links[slot].start()
-
-    lead_theirs = chunk_rows(jobs[0][2], 1 - core, 0)
-    lead_ours = chunk_rows(jobs[0][2], core, 0)
-    r.sib_send[slots] = dot(r.pool[lead_theirs, :], r.wop[...]).astype(BF16)
-    to_sibling(slots)
-    r.lead_pool[...] = dot(r.pool[lead_ours, :], r.wop[...])
-
-    def piece_spans(n):
-        return [slice(b * block + n * size, b * block + (n + 1) * size) for b in range(n_tp)]
-
-    def combine(h, n):
-        spans = piece_spans(n)
-        state = r.e_recv[h].reshape(HEAD_DIM, HEAD_DIM)
-        carried = dot(jnp.concatenate([r.q[h, span, :] for span in spans], axis=0), state)
-        squares = []
-        for b, span in enumerate(spans):
-            memory = r.num[h, span, :] + r.beta[h, span, :] * carried[b * size : (b + 1) * size]
-            r.num[h, span, :] = memory
-            squares.append(jnp.sum(memory * memory, axis=-1, keepdims=True))
-        squares = jnp.concatenate(squares, axis=0)
-        if h > 0:
-            squares = squares + jnp.concatenate([r.squares[span] for span in spans], axis=0)
-        r.sq_send[n] = jnp.broadcast_to(squares, (n_tp * size, 128)).T[0:1]
-
-    def combine_early(h):
+    def combine(h):
         state = r.e_recv[h].reshape(HEAD_DIM, HEAD_DIM)
         for t in range(tiles):
             span = slice(t * TILE, (t + 1) * TILE)
@@ -595,97 +645,77 @@
             squares = jnp.sum(memory * memory, axis=-1, keepdims=True)
             if h > 0:
                 squares = squares + r.squares[span]
-            r.squares[span] = squares
-
-    def square_copies(which):
-        pieces = slice(0, 1) if which == 0 else slice(1, CHUNKS)
-        made = []
+            if h < H - 1:
+                r.squares[span] = squares
+            else:
+                r.sq_send[:, span] = jnp.broadcast_to(squares, (TILE, 128)).T[0:1]
+
+    for h in range(H):
+        all_of(r.e_recv.at[h, pl.ds(0, quad - 1)], (r.e_sems.at[0, h], r.e_sems.at[1, h])).wait()
+        combine(h)
+    third = []
+    for step in range(1, n_tp):
+        third.append(
+            remote(
+                r.sq_send,
+                r.sq_recv.at[step],
+                r.sq_sems.at[0],
+                r.sq_sems.at[1],
+                "tp",
+                lax.rem(tp + step, n_tp),
+            )
+        )
+    for copy in third:
+        copy.start()
+    r.sib_send[place(1, 0), :] = memory_product(lead_theirs).astype(BF16)
+    to_sibling(1, 0)
+    r.lead[...] = memory_product(lead_ours)
+    pass_on(1, 0, first_target)
+    for j in range(1, chips):
+        gates_of(lax.rem(chip + j, chips))
+        pool_of(lax.rem(chip + j, chips))
+    all_of(r.sq_recv.at[pl.ds(0, n_tp - 1)], (r.sq_sems.at[0], r.sq_sems.at[1]), "tp").wait()
+    for t in range(tiles):
+        span = pl.ds(t * TILE, TILE)
+        total = r.sq_send[0:1, span]
         for step in range(1, n_tp):
-            made.append(
-                remote(
-                    r.sq_send.at[pieces],
-                    r.sq_recv.at[step, pieces],
-                    r.sq_sems.at[0, which, step],
-                    r.sq_sems.at[1, which, step],
-                    "tp",
-                    lax.rem(tp + step, n_tp),
-                )
-            )
-        return made
-
-    def scales(pieces):
-        for n in pieces:
-            total = r.sq_send[n]
-            for step in range(1, n_tp):
-                total = total + r.sq_recv[step, n]
-            scale = lax.rsqrt(total / (HEAD_DIM * H * n_tp) + EPS)
-            scale = jnp.broadcast_to(scale, (128, n_tp * size)).T
-            for b, span in enumerate(piece_spans(n)):
-                r.scale[span, :] = scale[b * size : (b + 1) * size]
-
-    for h in range(H):
-        for step in range(1, quad):
-            e_copy(h, step).wait()
-        if h < H - 1:
-            combine_early(h)
-    lead_squares, rest_squares = square_copies(0), square_copies(1)
-    combine(H - 1, 0)
-    for copy in lead_squares:
-        copy.start()
-    r.sib_send[0] = memory_product(lead_theirs).astype(BF16)
-    to_sibling(0)
-    for n in range(1, CHUNKS):
-        combine(H - 1, n)
-    for copy in rest_squares:
-        copy.start()
-    r.lead_memory[...] = memory_product(lead_ours)
-    for copy in lead_squares:
-        copy.wait()
-    scales([0])
-
-    siblings[slots].wait_recv()
-    siblings[0].wait_recv()
-    r.link_send[0] = (
-        (r.lead_memory[...] + r.sib_recv[0].astype(F32)) * r.scale[lead_ours, 0:1]
-        + r.lead_pool[...]
-        + r.sib_recv[slots].astype(F32)
-    ).astype(BF16)
-    to_chip(0, jobs[0][2])
-
-    def send_on(job):
-        j, n, target, slot = job
-        if j == chips:
-            return
-        siblings[slot].wait_recv()
-        r.link_send[slot] = (r.own[slot].astype(F32) + r.sib_recv[slot].astype(F32)).astype(BF16)
-        to_chip(slot, target)
-
-    for copy in rest_squares:
-        copy.wait()
-    scales(range(1, CHUNKS))
-    for index, (j, n, target, slot) in enumerate(jobs):
+            total = total + r.sq_recv[step, 0:1, span]
+        scale = lax.rsqrt(total / (HEAD_DIM * H * n_tp) + EPS)
+        r.scale[span, :] = jnp.broadcast_to(scale, (128, TILE)).T
+
+    for index, (j, n, target) in enumerate(jobs):
         if index == 0:
             continue
         if j == chips and n == 0:
             gates_of(chip)
             pool_of(chip)
-        r.sib_send[slot] = finish(chunk_rows(target, 1 - core, n))
-        to_sibling(slot)
-        r.own[slot] = finish(chunk_rows(target, core, n))
-        if index > 1:
-            send_on(jobs[index - 1])
-    outs = []
-    for n in range(CHUNKS):
-        slot = (chips - 1) * CHUNKS + n
-        siblings[slot].wait_recv()
-        total = r.own[slot].astype(F32) + r.sib_recv[slot].astype(F32)
+        r.sib_send[place(j, n), :] = finish(chunk_rows(target, 1 - core, n))
+        to_sibling(j, n)
+        r.own[place(j, n), :] = finish(chunk_rows(target, core, n))
+        if index == 1 and j < chips:
+            pass_on(j, n, target)
+        elif index > 2 and jobs[index - 1][0] < chips:
+            pass_on(*jobs[index - 1])
+    own_scale = r.scale.at[pl.ds(pl.multiple_of(tp * block, block), lead)]
+    for n in range(count):
+        siblings[chips, n].wait_recv()
+        begin, size = chunks[n]
+        total = r.own[place(chips, n), :].astype(F32) + r.sib_recv[place(chips, n), :].astype(F32)
         for j in range(1, chips):
-            other = (j - 1) * CHUNKS + n
-            links[other].wait_recv()
-            total = total + r.link_recv[other].astype(F32)
+            links[j, n].wait_recv()
+            came = r.link_recv[place(j, n), :].astype(F32)
+            if (j, n) == (1, 0):
+                links[1, -1].wait_recv()
+                came = came * own_scale[:, 0:1] + r.link_recv[place(1, -1), :].astype(F32)
+            total = total + came
         scale = lax.rsqrt(jnp.mean(total * total, axis=-1, keepdims=True) + EPS)
-        span = pl.ds(n * size, size)
-        out_hbm[span, :] = (total * scale * r.post[...]).astype(BF16)
+        out_ref[begin : begin + size, :] = (total * scale * r.post[...]).astype(BF16)
+    for member in range(n_tp):
+
+        @pl.when((tp == member) & (sp < n_sp - 1))
+        def _(member=member):
+            halo_copy(member).wait_send()
+
 
     @pl.when(owner != sp)
     def _():
@@ -696,10 +726,10 @@
         def _(h=h):
             t_copy(h).wait_send()
 
-    for copy in [*siblings.values(), *links.values()]:
-        copy.wait_send()
-    for copy in outs:
-        copy.wait()
+    sent = r.sib_send.at[pl.ds(0, chips * block + lead)]
+    all_of(sent, (r.sib_sems.at[extra_slot + 1], r.sib_sems.at[0]), "tp").wait_send()
+    sent = r.link_send.at[pl.ds(0, (chips - 1) * block + lead)]
+    all_of(sent, (r.link_sems.at[extra_slot - count + 1], r.link_sems.at[0]), "tp").wait_send()
 
 
 def body(
@@ -738,8 +768,8 @@
     rows_own = HEAD_DIM // quad
     chips = n_tp // 2
     block = T // n_tp
-    slots = chips * CHUNKS
-    size = block // CHUNKS
+    slots = chips * len(SHARES)
+    lead = block // sum(SHARES) * SHARES[0]
     hbm = pl.BlockSpec(memory_space=pl.ANY)
     V = pltpu.VMEM
     dma = pltpu.SemaphoreType.DMA
@@ -793,26 +823,25 @@
         t_send=V((H, rows_own, HEAD_DIM), BF16),
         t_recv=V((H, rows_own, HEAD_DIM), BF16),
         squares=V((T, 1), F32),
-        sq_send=V((CHUNKS, 1, T // CHUNKS), F32),
-        sq_recv=V((n_tp, CHUNKS, 1, T // CHUNKS), F32),
-        lead_pool=V((size, D), F32),
-        lead_memory=V((size, D), F32),
+        sq_send=V((1, T), F32),
+        sq_recv=V((n_tp, 1, T), F32),
+        lead=V((lead, D), F32),
         scale=V((T, 128), F32),
-        sib_send=V((slots + 1, size, D), BF16),
-        sib_recv=V((slots + 1, size, D), BF16),
-        own=V((slots, size, D), BF16),
-        link_send=V((slots, size, D), BF16),
-        link_recv=V((slots, size, D), BF16),
-        local_sem=dma((INPUTS + T // TILE + 2 * H,)),
+        sib_send=V((chips * block + lead, D), BF16),
+        sib_recv=V((chips * block + lead, D), BF16),
+        own=V((chips * block, D), BF16),
+        link_send=V((chips * block + lead, D), BF16),
+        link_recv=V((chips * block + lead, D), BF16),
+        local_sem=dma((INPUTS - 8 + T // TILE + 2 * H,)),
         init_sems=dma((n_sp // quad + 1,)),
-        a_sems=dma((2, H, n_sp)),
-        s_sems=dma((2, H, quad)),
-        e_sems=dma((2, H, quad)),
+        a_sems=dma((2, H)),
+        s_sems=dma((2, H)),
+        e_sems=dma((2, H)),
         t_sems=dma((2, H)),
         halo_sems=dma((2,)),
-        sq_sems=dma((2, 2, n_tp)),
-        sib_sems=dma((2, slots + 1)),
-        link_sems=dma((2, slots)),
+        sq_sems=dma((2,)),
+        sib_sems=dma((slots + 2,)),
+        link_sems=dma((slots - len(SHARES) + 2,)),
     )
     return pl.pallas_call(
         functools.partial(kernel, n_sp, n_tp, tuple(scratch)),

time: 57.7 us -> 53.3 us (0.924)
  Pallas kernels: 56.5 us -> 52.1 us
    pallas_call x1, Pallas kernels: 56.5 us -> 52.1 us  [body(): pl.pallas_call(functools.partial(kernel, n_sp, n_tp, tuple(scratch)), out...]
where the time goes in v2:
time: 53.3 us; the launch traced here: 53.1 us
  Pallas kernels  52.1 us (98%)
  local copies, waits for them, and re-layouts  0.97 us (2%)
    pallas_call x1, Pallas kernels, body(): pl.pallas_call(functools.partial(kernel, n_sp, n_tp, tuple(scratch)), out...  52.1 us

profile of v2, /device:TPU:0, one launch (start us, length us, event | category | flops | bytes accessed | tf_op | source)
XLA Modules:
  0.0 53.1 jit_solution(12247730909156022979)
XLA Ops:
  0.0 52.1 %shard_map.199 = bf16[256,2048]{1,0:T(8,128)(2,1)S(1)} custom-call(bf16[1024,2048]{1,0:T(8,128)(2,1)} %refs_0_.1, f32[1,2048]{1,0:T(1,128)} %bitcast.11, bf16[2048,512]{1,0:T(8,128)(2,1)} %refs_2_.1, bf16[2048,512]{1,0:T(8,128)(2,1)} %refs_3_.1, bf16[2048,512]{1,0:T(8,128)(2,1)} %refs_4_.1, bf16[2048,512]{1,0:T(8,128)(2,1)} %refs_5_.1, ...), custom_call_target="tpu_custom_call" | custom-call | tf_op jit(solution)/shard_map/pallas_call | solution.py:846
  52.1 1.0 %copy.23 = bf16[256,2048]{1,0:T(8,128)(2,1)} copy(bf16[256,2048]{1,0:T(8,128)(2,1)S(1)} %shard_map.199) | data formatting | bytes 2097152

commit v3 on v2

--- a/solution.py
+++ b/solution.py
@@ -532,10 +532,16 @@
         def _(member=member):
             halo_copy(member).wait_recv()
 
-    for which in (1 - core, core):
+    def lead_pool(which):
         pool_rows(pl.multiple_of((first_target * 2 + which) * block, block), lead)
-    def memory_product(rows):
-        parts = [(r.num[h, rows, :] * r.gate[h, rows, :]).astype(BF16) for h in range(H)]
+
+    lead_pool(1 - core)
+    def memory_product(rows, entering=None):
+        values = [r.num[h, rows, :] for h in range(H)]
+        if entering is not None:
+            carried = dot(r.q[H - 1, rows, :], entering)
+            values[-1] = values[-1] + r.beta[H - 1, rows, :] * carried
+        parts = [(values[h] * r.gate[h, rows, :]).astype(BF16) for h in range(H)]
         return dot(parts[0] if H == 1 else jnp.concatenate(parts, axis=1), r.wom[...])
 
     def finish(rows):
@@ -583,6 +589,7 @@
 
     r.sib_send[place(1, -1), :] = dot(r.pool[lead_theirs, :], r.wop[...]).astype(BF16)
     to_sibling(1, -1)
+    lead_pool(core)
     r.lead[...] = dot(r.pool[lead_ours, :], r.wop[...])
 
     def pass_on(j, n, target):
@@ -597,10 +604,10 @@
         jnp.int32, (TILE, TILE), 1
     )
 
-    def attend(h):
+    def attend(h, members):
         enter_max = r.enter[h : h + 1, 0:1]
         enter_normal = r.enter[H + h : H + h + 1, :]
-        for t in range(tiles):
+        for t in members:
             span = pl.ds(t * TILE, TILE)
             queries = r.q[h, span, :]
             near = jnp.where(diag_mask, r.rows[h : h + 1, span], FLOOR)
@@ -628,13 +635,14 @@
             r.num[h, span, :] = num * (local_weight / bound)
             r.beta[h, span, :] = carry_weight / bound
 
-    attend(0)
+    attend(0, range(tiles // 2))
     pass_on(1, -1, first_target)
+    attend(0, range(tiles // 2, tiles))
     for h in range(1, H):
         carried_on(h)
 
     for h in range(1, H):
-        attend(h)
+        attend(h, range(tiles))
     def combine(h):
         state = r.e_recv[h].reshape(HEAD_DIM, HEAD_DIM)
         for t in range(tiles):
@@ -652,23 +660,21 @@
 
     for h in range(H):
         all_of(r.e_recv.at[h, pl.ds(0, quad - 1)], (r.e_sems.at[0, h], r.e_sems.at[1, h])).wait()
-        combine(h)
-    third = []
+        if h < H - 1:
+            combine(h)
+    entering = r.e_recv[H - 1].reshape(HEAD_DIM, HEAD_DIM)
+    r.sib_send[place(1, 0), :] = memory_product(lead_theirs, entering).astype(BF16)
+    to_sibling(1, 0)
+    combine(H - 1)
     for step in range(1, n_tp):
-        third.append(
-            remote(
-                r.sq_send,
-                r.sq_recv.at[step],
-                r.sq_sems.at[0],
-                r.sq_sems.at[1],
-                "tp",
-                lax.rem(tp + step, n_tp),
-            )
-        )
-    for copy in third:
-        copy.start()
-    r.sib_send[place(1, 0), :] = memory_product(lead_theirs).astype(BF16)
-    to_sibling(1, 0)
+        remote(
+            r.sq_send,
+            r.sq_recv.at[step],
+            r.sq_sems.at[0],
+            r.sq_sems.at[1],
+            "tp",
+            lax.rem(tp + step, n_tp),
+        ).start()
     r.lead[...] = memory_product(lead_ours)
     pass_on(1, 0, first_target)
     for j in range(1, chips):

time: 53.3 us -> 53.1 us (level)
  no operation moved by 1% of the time
where the time goes in v3:
time: 53.1 us; the launch traced here: 52.9 us
  Pallas kernels  51.9 us (98%)
  local copies, waits for them, and re-layouts  0.97 us (2%)
    pallas_call x1, Pallas kernels, body(): pl.pallas_call(functools.partial(kernel, n_sp, n_tp, tuple(scratch)), out...  51.9 us

profile of v3, /device:TPU:0, one launch (start us, length us, event | category | flops | bytes accessed | tf_op | source)
XLA Modules:
  0.0 52.9 jit_solution(1885635295244714030)
XLA Ops:
  0.0 51.9 %shard_map.199 = bf16[256,2048]{1,0:T(8,128)(2,1)S(1)} custom-call(bf16[1024,2048]{1,0:T(8,128)(2,1)} %refs_0_.1, f32[1,2048]{1,0:T(1,128)} %bitcast.11, bf16[2048,512]{1,0:T(8,128)(2,1)} %refs_2_.1, bf16[2048,512]{1,0:T(8,128)(2,1)} %refs_3_.1, bf16[2048,512]{1,0:T(8,128)(2,1)} %refs_4_.1, bf16[2048,512]{1,0:T(8,128)(2,1)} %refs_5_.1, ...), custom_call_target="tpu_custom_call" | custom-call | tf_op jit(solution)/shard_map/pallas_call | solution.py:852
  51.9 1.0 %copy.23 = bf16[256,2048]{1,0:T(8,128)(2,1)} copy(bf16[256,2048]{1,0:T(8,128)(2,1)S(1)} %shard_map.199) | data formatting | bytes 2097152
